TPU v7x, 32 devices: a whole 2x2x4 slice. The times are simulated.
32 devices in a mesh: kv: 8 (over z, x), tp: 4 (over y, core).
Axes of the slice: x: 2, y: 2, z: 4, core: 2. Of those that a mesh axis runs over, the one named last changes fastest.
Arguments:
- tokens: bfloat16 [64, 12, 4096], P(None, None, 'kv'), may hold values from -6 to 6
- parents: int32 [64, 12], P('kv'), may hold values from -1 to 10, as said below
- accepted: int32 [64], P('kv'), may hold values from 0 to 6
- state: float32 [64, 64, 64, 128], P('kv', 'tp'), may hold values from -4 to 4
- conv_x: bfloat16 [64, 3, 4096], P('kv', None, 'tp'), may hold values from -6 to 6
- conv_b: bfloat16 [64, 3, 2048], P('kv', None, 'tp'), may hold values from -6 to 6
- conv_c: bfloat16 [64, 3, 2048], P('kv', None, 'tp'), may hold values from -6 to 6
- path_x: bfloat16 [64, 6, 4096], P('kv', None, 'tp'), may hold values from -6 to 6
- path_b: bfloat16 [64, 6, 2048], P('kv', None, 'tp'), may hold values from -6 to 6
- path_c: bfloat16 [64, 6, 2048], P('kv', None, 'tp'), may hold values from -6 to 6
- path_dt: bfloat16 [64, 6, 64], P('kv', None, 'tp'), may hold values from -6 to 6
- gain_in: float32 [4096], replicated, may hold values from 0.1 to 1.9
- w_x: bfloat16 [4096, 4096], P('kv', 'tp'), may hold values from -0.09375 to 0.09375
- w_z: bfloat16 [4096, 4096], P('kv', 'tp'), may hold values from -0.09375 to 0.09375
- w_b: bfloat16 [4096, 2048], P('kv', 'tp'), may hold values from -0.09375 to 0.09375
- w_c: bfloat16 [4096, 2048], P('kv', 'tp'), may hold values from -0.09375 to 0.09375
- w_dt: bfloat16 [4096, 64], replicated, may hold values from -0.09375 to 0.09375
- dt_bias: float32 [64], P('tp'), may hold values from -2 to 1
- a_log: float32 [64], P('tp'), may hold values from -3 to 1.5
- d_skip: float32 [64], P('tp'), may hold values from 0.5 to 1.5
- conv_wx: bfloat16 [4, 4096], P(None, 'tp'), may hold values from -3 to 3
- conv_wb: bfloat16 [4, 2048], P(None, 'tp'), may hold values from -3 to 3
- conv_wc: bfloat16 [4, 2048], P(None, 'tp'), may hold values from -3 to 3
- gain_out: float32 [4096], P('tp'), may hold values from 0.1 to 1.9
- w_out: bfloat16 [4096, 4096], P('tp', 'kv'), may hold values from -0.09375 to 0.09375
Outputs:
- mixed: bfloat16 [64, 12, 4096], P('kv', None, 'tp')
- new_state: float32 [64, 64, 64, 128], P('kv', 'tp')
Inputs may be any that keep to these rules, and one draw needn't show every extreme that they name: `parents`: each proposal's parent is -1 or an earlier proposal of the same sequence; the first proposal's parent is -1.
All inputs are finite; a program needn't handle non-finite values.
Results may differ from a plain program's by a relative error of at most 0.03.
Values may be sent and summed in bfloat16 or wider, within the bound.
A program may use at most 128 MiB of HBM per device.

v0:
```python
import functools

import jax
import jax.numpy as jnp
from jax import lax
from jax.experimental import pallas as pl
from jax.experimental.pallas import tpu as pltpu
from jax.sharding import PartitionSpec as P

HPG = 4


EPS = 1e-06
HIGH = lax.Precision.HIGHEST
MESH = pl.DeviceIdType.MESH


def inner_size(ranks):
    return max(d for d in range(1, ranks + 1) if ranks % d == 0 and d * d <= ranks)


def scatter_kernel(
    near,
    far,
    width,
    square_column,
    part_ref,
    side_ref,
    rows_ref,
    rate_ref,
    near_main,
    near_side,
    sum_main,
    sum_side,
    pair_main,
    pair_side,
    pass_main,
    pass_side,
    far_main,
    far_side,
    near_sends,
    near_recvs,
    pair_sends,
    pair_recvs,
    far_sends,
    far_recvs,
):
    mine = lax.axis_index("kv")
    column = lax.axis_index("tp")
    my_far = mine // near
    my_near = lax.rem(mine, near)
    partner = my_far + 1 - 2 * lax.rem(my_far, 2)
    half = far // 2

    def place(home, jump, step_near):
        return lax.rem(home + 2 * jump, far) * near + lax.rem(my_near + step_near, near)

    barrier = pltpu.get_barrier_semaphore()
    peers = [place(my_far, 0, step) for step in range(1, near)]
    peers = peers + [place(partner, 0, 0)]
    peers = peers + [place(my_far, jump, 0) for jump in range(1, half)]
    for peer in peers:
        pl.semaphore_signal(barrier, inc=1, device_id=(peer, column), device_id_type=MESH)
    pl.semaphore_wait(barrier, len(peers))

    order = [(jump, kind) for jump in list(range(1, half)) + [0] for kind in range(2)]
    homes = (partner, my_far)
    near_copies = {}

    def start_near(jump, kind):
        slot = 2 * jump + kind
        for step in range(1, near):
            for which, (source, landing) in enumerate(
                ((side_ref, near_side), (part_ref, near_main))
            ):
                copy = pltpu.make_async_remote_copy(
                    src_ref=source.at[place(homes[kind], jump, step)],
                    dst_ref=landing.at[slot, step - 1],
                    send_sem=near_sends.at[which, slot, step - 1],
                    recv_sem=near_recvs.at[which, slot, step - 1],
                    device_id=(place(my_far, 0, step), column),
                    device_id_type=MESH,
                )
                copy.start()
                near_copies[slot, step, which] = copy

    start_near(*order[0])
    columns = rows_ref.shape[1]
    chunk = 512 if columns % 512 == 0 else columns

    def add_up(block, slot, extra_main, extra_side, put_side, put_main):
        side = side_ref[block].astype(jnp.float32)
        for step in range(1, near):
            side = side + near_side[slot, step - 1].astype(jnp.float32)
        for ref, place_of in extra_side:
            side = side + ref[place_of].astype(jnp.float32)
        state = put_side(side)

        @pl.loop(0, columns // chunk)
        def _(turn):
            span = pl.ds(pl.multiple_of(turn * chunk, chunk), chunk)
            total = part_ref[block, :, span].astype(jnp.float32)
            for step in range(1, near):
                total = total + near_main[slot, step - 1, :, span].astype(jnp.float32)
            for ref, place_of in extra_main:
                total = total + ref[place_of, :, span].astype(jnp.float32)
            put_main(span, total, state)

    def send(refs, sems, source_at, target):
        made = []
        for which, (source, landing) in enumerate(refs):
            copy = pltpu.make_async_remote_copy(
                src_ref=source.at[source_at],
                dst_ref=landing.at[source_at],
                send_sem=sems[0].at[which, source_at],
                recv_sem=sems[1].at[which, source_at],
                device_id=(target, column),
                device_id_type=MESH,
            )
            copy.start()
            made.append(copy)
        return made

    def keep_side(ref, at):
        def put(side):
            ref[at] = side.astype(ref.dtype)

        return put

    def keep_main(ref, at):
        def put(span, total, state):
            ref[at, :, span] = total.astype(ref.dtype)

        return put

    pair_copies = {}
    far_copies = []
    for turn, (jump, kind) in enumerate(order):
        slot = 2 * jump + kind
        for step in range(1, near):
            for which in range(2):
                near_copies[slot, step, which].wait_recv()
        if turn + 1 < len(order):
            start_near(*order[turn + 1])
        if kind == 0:
            add_up(
                place(partner, jump, 0),
                slot,
                [],
                [],
                keep_side(sum_side, jump),
                keep_main(sum_main, jump),
            )
            pair_copies[jump] = send(
                ((sum_side, pair_side), (sum_main, pair_main)),
                (pair_sends, pair_recvs),
                jump,
                place(partner, 0, 0),
            )
            continue
        for copy in pair_copies[jump]:
            copy.wait_recv()
        if jump > 0:
            target = place(my_far, jump, 0)
            add_up(
                target,
                slot,
                [(pair_main, jump)],
                [(pair_side, jump)],
                keep_side(pass_side, jump - 1),
                keep_main(pass_main, jump - 1),
            )
            far_copies = far_copies + send(
                ((pass_side, far_side), (pass_main, far_main)),
                (far_sends, far_recvs),
                jump - 1,
                target,
            )
    for copy in far_copies:
        copy.wait()
    for made in pair_copies.values():
        for copy in made:
            copy.wait_send()
    for copy in near_copies.values():
        copy.wait_send()

    def last_side(side):
        row_scale = lax.rsqrt(side[:, square_column : square_column + 1] / width + EPS)
        rate_ref[...] = (side * row_scale).astype(rate_ref.dtype)
        return row_scale

    def last_main(span, total, row_scale):
        rows_ref[:, span] = (total * row_scale).astype(rows_ref.dtype)

    add_up(
        mine,
        1,
        [(pair_main, 0)] + [(far_main, jump) for jump in range(half - 1)],
        [(pair_side, 0)] + [(far_side, jump) for jump in range(half - 1)],
        last_side,
        last_main,
    )


def scatter_rows(part, side, width, square_column):
    ranks, rows, columns = part.shape
    side_columns = side.shape[2]
    near = inner_size(ranks)
    far = ranks // near
    vmem = pl.BlockSpec(memory_space=pltpu.VMEM)
    return pl.pallas_call(
        functools.partial(scatter_kernel, near, far, width, square_column),
        out_shape=(
            jax.ShapeDtypeStruct((rows, columns), jnp.bfloat16),
            jax.ShapeDtypeStruct((rows, side_columns), jnp.bfloat16),
        ),
        in_specs=[vmem, vmem],
        out_specs=(vmem, vmem),
        scratch_shapes=[
            pltpu.VMEM((far, near - 1, rows, columns), jnp.bfloat16),
            pltpu.VMEM((far, near - 1, rows, side_columns), jnp.bfloat16),
            pltpu.VMEM((far // 2, rows, columns), jnp.bfloat16),
            pltpu.VMEM((far // 2, rows, side_columns), jnp.bfloat16),
            pltpu.VMEM((far // 2, rows, columns), jnp.bfloat16),
            pltpu.VMEM((far // 2, rows, side_columns), jnp.bfloat16),
            pltpu.VMEM((far // 2 - 1, rows, columns), jnp.bfloat16),
            pltpu.VMEM((far // 2 - 1, rows, side_columns), jnp.bfloat16),
            pltpu.VMEM((far // 2 - 1, rows, columns), jnp.bfloat16),
            pltpu.VMEM((far // 2 - 1, rows, side_columns), jnp.bfloat16),
            pltpu.SemaphoreType.DMA((2, far, near - 1)),
            pltpu.SemaphoreType.DMA((2, far, near - 1)),
            pltpu.SemaphoreType.DMA((2, far // 2)),
            pltpu.SemaphoreType.DMA((2, far // 2)),
            pltpu.SemaphoreType.DMA((2, far // 2 - 1)),
            pltpu.SemaphoreType.DMA((2, far // 2 - 1)),
        ],
        compiler_params=pltpu.CompilerParams(collective_id=0, has_side_effects=True),
    )(part, side)


def out_kernel(
    ranks,
    blocks,
    gated_ref,
    w_ref,
    mixed_ref,
    gathered,
    terms,
    landed,
    gather_sends,
    gather_recvs,
    term_sends,
    term_recvs,
):
    mine = lax.axis_index("kv")
    column = lax.axis_index("tp")
    ratio = ranks // blocks
    owner = mine // ratio
    place = lax.rem(mine, ratio)
    slab = w_ref.shape[1]
    barrier = pltpu.get_barrier_semaphore()
    for offset in range(1, ranks):
        pl.semaphore_signal(
            barrier,
            inc=1,
            device_id=(lax.rem(mine + offset, ranks), column),
            device_id_type=MESH,
        )
    for near in range(ratio):
        source = column * ratio + near
        for block in range(blocks):

            @pl.when(block != column)
            def _():
                pl.semaphore_signal(
                    barrier, inc=1, device_id=(source, block), device_id_type=MESH
                )

    @pl.when(owner == column)
    def _():
        pl.semaphore_wait(barrier, ranks - 1)

    @pl.when(owner != column)
    def _():
        pl.semaphore_wait(barrier, 2 * ranks - 1)

    inner = inner_size(ranks)
    outer = ranks // inner
    my_outer = mine // inner
    my_inner = lax.rem(mine, inner)

    def spot(step_outer, step_inner):
        return lax.rem(my_outer + step_outer, outer) * inner + lax.rem(
            my_inner + step_inner, inner
        )

    copies = {}

    def gather_copy(source, offset, target):
        copy = pltpu.make_async_remote_copy(
            src_ref=source,
            dst_ref=gathered.at[offset - 1],
            send_sem=gather_sends.at[offset - 1],
            recv_sem=gather_recvs.at[offset - 1],
            device_id=(target, column),
            device_id_type=MESH,
        )
        copy.start()
        copies[offset] = copy

    for step in range(1, outer):
        gather_copy(gated_ref, step * inner, spot(step, 0))
    for step in range(1, inner):
        gather_copy(gated_ref, step, spot(0, step))

    def term_copy(offset, target):
        return pltpu.make_async_remote_copy(
            src_ref=terms.at[offset],
            dst_ref=landed.at[place, column],
            send_sem=term_sends.at[offset],
            recv_sem=term_recvs.at[place, column],
            device_id=(target, owner),
            device_id_type=MESH,
        )

    def origin(offset):
        return spot(outer - offset // inner, inner - offset % inner)

    turns = [0] + [step * inner for step in range(1, outer)]
    turns = turns + [offset for offset in range(ranks) if offset % inner]
    for offset in turns:
        target = origin(offset)
        if offset == 0:
            block = gated_ref[...]
        else:
            copies[offset].wait_recv()
            if offset % inner == 0:
                for step in range(1, inner):
                    gather_copy(gathered.at[offset - 1], offset + step, spot(0, step))
            block = gathered[offset - 1]
        term = jnp.dot(block, w_ref[...], preferred_element_type=jnp.float32).astype(
            jnp.bfloat16
        )
        if offset == 0:

            @pl.when(owner == column)
            def _():
                landed[place, column] = term

            @pl.when(owner != column)
            def _():
                terms[0] = term
                term_copy(0, target).start()

        else:
            terms[offset] = term
            term_copy(offset, target).start()

    for near in range(ratio):
        source = column * ratio + near
        for block in range(blocks):

            @pl.when(jnp.logical_or(source != mine, block != column))
            def _():
                pltpu.make_async_remote_copy(
                    src_ref=terms.at[0],
                    dst_ref=landed.at[near, block],
                    send_sem=term_sends.at[0],
                    recv_sem=term_recvs.at[near, block],
                    device_id=(source, block),
                    device_id_type=MESH,
                ).wait_recv()

        total = landed[near, 0].astype(jnp.float32)
        for block in range(1, blocks):
            total = total + landed[near, block].astype(jnp.float32)
        mixed_ref[:, near * slab : (near + 1) * slab] = total.astype(mixed_ref.dtype)
    for offset in range(ranks):
        target = origin(offset)
        if offset == 0:

            @pl.when(owner != column)
            def _():
                term_copy(0, target).wait_send()

        else:
            copies[offset].wait_send()
            term_copy(offset, target).wait_send()


def project_out(gated, w_out, ranks, blocks):
    rows = gated.shape[0]
    inner, slab = w_out.shape
    ratio = ranks // blocks
    vmem = pl.BlockSpec(memory_space=pltpu.VMEM)
    return pl.pallas_call(
        functools.partial(out_kernel, ranks, blocks),
        out_shape=jax.ShapeDtypeStruct((rows, ratio * slab), jnp.bfloat16),
        in_specs=[vmem, vmem],
        out_specs=vmem,
        scratch_shapes=[
            pltpu.VMEM((ranks - 1, rows, inner), jnp.bfloat16),
            pltpu.VMEM((ranks, rows, slab), jnp.bfloat16),
            pltpu.VMEM((ratio, blocks, rows, slab), jnp.bfloat16),
            pltpu.SemaphoreType.DMA((ranks - 1,)),
            pltpu.SemaphoreType.DMA((ranks - 1,)),
            pltpu.SemaphoreType.DMA((ranks,)),
            pltpu.SemaphoreType.DMA((ratio, blocks)),
        ],
        compiler_params=pltpu.CompilerParams(collective_id=1, has_side_effects=True),
    )(gated, w_out)


def conv_window(history, taps, amount):
    values = history.astype(jnp.float32)
    weights = taps.astype(jnp.float32)
    summed = weights[0] * values[:, 0:amount, :]
    for distance in range(1, weights.shape[0]):
        summed = summed + weights[distance] * values[:, distance : distance + amount, :]
    return jax.nn.silu(summed)


def commit_rows(history, accepted, keep):
    picked = accepted[:, None] + jnp.arange(keep, dtype=jnp.int32)[None, :]
    select = (
        picked[:, :, None] == jnp.arange(history.shape[1], dtype=jnp.int32)[None, None, :]
    ).astype(jnp.float32)
    return jnp.einsum("skl,slc->skc", select, history.astype(jnp.float32), precision=HIGH).astype(
        jnp.bfloat16
    )


def replay_state(
    state, history_x, history_b, path_dt, conv_wx, conv_wb, accepted, rate_bias, a_rate, per_group
):
    seq_count, heads, head_dim, state_dim = state.shape
    path_len = path_dt.shape[1]
    path_xs = conv_window(history_x, conv_wx, path_len).reshape(
        seq_count, path_len, heads, head_dim
    )
    path_bs = conv_window(history_b, conv_wb, path_len).reshape(
        seq_count, path_len, heads // per_group, state_dim
    )
    path_bh = jnp.repeat(path_bs, per_group, axis=2)
    path_step = jax.nn.softplus(path_dt.astype(jnp.float32) + rate_bias)
    is_live = (jnp.arange(path_len, dtype=jnp.int32)[None, :] < accepted[:, None]).astype(
        jnp.float32
    )[:, :, None]
    log_decay = path_step * a_rate * is_live
    overall = jnp.sum(log_decay, axis=1)
    tail_sum = overall[:, None, :] - jnp.cumsum(log_decay, axis=1)
    weights = is_live * jnp.exp(tail_sum) * path_step
    grown = jnp.einsum("sjh,sjhp,sjhn->shpn", weights, path_xs, path_bh, precision=HIGH)
    return jnp.exp(overall)[:, :, None, None] * state + grown


def tree_links(parents, keep):
    seq_count, prop_count = parents.shape
    front = jnp.broadcast_to(jnp.arange(-1, keep - 1, dtype=jnp.int32)[None, :], (seq_count, keep))
    parent_ids = jnp.concatenate([front, parents + keep], axis=1)
    nodes = keep + prop_count
    links = (parent_ids[:, :, None] == jnp.arange(nodes, dtype=jnp.int32)[None, None, :]).astype(
        jnp.float32
    )
    identity = jnp.eye(prop_count, dtype=jnp.float32)[None, :, :]
    ancestry = identity + links[:, keep:, keep:]
    for turn in range(prop_count.bit_length()):
        ancestry = jnp.minimum(jnp.einsum("sij,sjk->sik", ancestry, ancestry, precision=HIGH), 1.0)
    return (links, ancestry)


def tree_conv(buffer, rows, taps, links, keep):
    values = jnp.concatenate([buffer, rows], axis=1).astype(jnp.float32)
    weights = taps.astype(jnp.float32)
    last_tap = weights.shape[0] - 1
    summed = weights[last_tap] * values
    reached = values
    for distance in range(1, last_tap + 1):
        reached = jnp.einsum("sij,sjc->sic", links, reached, precision=HIGH)
        summed = summed + weights[last_tap - distance] * reached
    return jax.nn.silu(summed[:, keep:, :])


def tree_mix(
    state,
    post_x,
    post_b,
    post_c,
    rate_rows,
    z_rows,
    ancestry,
    rate_bias,
    a_rate,
    d_skip,
    gain_out,
    per_group,
):
    seq_count, prop_count, _ = post_x.shape
    heads, head_dim, state_dim = (state.shape[1], state.shape[2], state.shape[3])
    groups = heads // per_group
    x_heads = post_x.reshape(seq_count, prop_count, heads, head_dim)
    b_groups = post_b.reshape(seq_count, prop_count, groups, state_dim)
    c_groups = post_c.reshape(seq_count, prop_count, groups, state_dim)
    step_size = jax.nn.softplus(rate_rows.astype(jnp.float32) + rate_bias)
    path_decay = jnp.einsum("sij,sjh->sih", ancestry, step_size * a_rate, precision=HIGH)
    c_heads = jnp.repeat(c_groups, per_group, axis=2)
    carried = (
        jnp.einsum("sihn,shpn->sihp", c_heads, state, precision=HIGH)
        * jnp.exp(path_decay)[:, :, :, None]
    )
    scores = jnp.einsum("sign,sjgn->sgij", c_groups, b_groups, precision=HIGH)
    scores = jnp.repeat(scores, per_group, axis=1)
    decay_t = jnp.transpose(path_decay, (0, 2, 1))
    decay_gap = decay_t[:, :, :, None] - decay_t[:, :, None, :]
    is_live = ancestry[:, None, :, :] > 0.5
    mixing = jnp.where(is_live, jnp.exp(jnp.where(is_live, decay_gap, 0.0)), 0.0)
    mixing = mixing * jnp.transpose(step_size, (0, 2, 1))[:, :, None, :]
    within = jnp.einsum("shij,sjhp->sihp", scores * mixing, x_heads, precision=HIGH)
    heads_out = carried + within + d_skip[None, None, :, None] * x_heads
    heads_out = heads_out.reshape(seq_count, prop_count, heads * head_dim) * jax.nn.silu(
        z_rows.astype(jnp.float32)
    )
    grouped = heads_out.reshape(seq_count, prop_count, groups, per_group * head_dim)
    grouped = grouped * lax.rsqrt(jnp.mean(grouped * grouped, axis=-1, keepdims=True) + EPS)
    return (grouped.reshape(seq_count, prop_count, heads * head_dim) * gain_out).astype(
        jnp.bfloat16
    )


def shards(
    tokens,
    parents,
    accepted,
    state,
    conv_x,
    conv_b,
    conv_c,
    path_x,
    path_b,
    path_c,
    path_dt,
    gain_in,
    w_x,
    w_z,
    w_b,
    w_c,
    w_dt,
    dt_bias,
    a_log,
    d_skip,
    conv_wx,
    conv_wb,
    conv_wc,
    gain_out,
    w_out,
):
    seq_local = state.shape[0]
    proposals = parents.shape[1]
    heads_local = dt_bias.shape[0]
    inner_local = w_x.shape[1]
    group_cols = w_b.shape[1]
    width = gain_in.shape[0]
    keep = conv_wx.shape[0] - 1
    tp_index = lax.axis_index("tp")
    kv_index = lax.axis_index("kv")
    slab_width = tokens.shape[2]
    flat_rows = tokens.reshape(-1, slab_width).astype(jnp.float32)
    gain_part = lax.dynamic_slice_in_dim(gain_in, kv_index * slab_width, slab_width)
    scaled = (flat_rows * gain_part).astype(jnp.bfloat16)
    w_joined = jnp.concatenate([w_x, w_z, w_b, w_c], axis=1)
    ranks = lax.axis_size("kv")
    blocks = lax.axis_size("tp")
    part = jnp.dot(scaled, w_joined, preferred_element_type=jnp.float32).astype(jnp.bfloat16)
    w_rate = lax.dynamic_slice(
        w_dt, (kv_index * slab_width, tp_index * heads_local), (slab_width, heads_local)
    )
    rate_term = jnp.dot(scaled, w_rate, preferred_element_type=jnp.float32)
    squares = jnp.sum(flat_rows * flat_rows, axis=1, keepdims=True)
    side = jnp.concatenate([rate_term, squares], axis=1).astype(jnp.bfloat16)
    side = jnp.pad(side, ((0, 0), (0, -side.shape[1] % 128)))
    rows_all, rate_all = scatter_rows(
        part.reshape(ranks, -1, part.shape[1]),
        side.reshape(ranks, -1, side.shape[1]),
        width,
        heads_local,
    )

    def column_part(lower, upper):
        return rows_all[:, lower:upper].reshape(seq_local, proposals, upper - lower)

    x_rows = column_part(0, inner_local)
    z_rows = column_part(inner_local, 2 * inner_local)
    b_rows = column_part(2 * inner_local, 2 * inner_local + group_cols)
    c_rows = column_part(2 * inner_local + group_cols, 2 * inner_local + 2 * group_cols)
    rate_rows = rate_all[:, :heads_local].reshape(seq_local, proposals, heads_local)
    a_rate = -jnp.exp(a_log)
    history_x = jnp.concatenate([conv_x, path_x], axis=1)
    history_b = jnp.concatenate([conv_b, path_b], axis=1)
    history_c = jnp.concatenate([conv_c, path_c], axis=1)
    new_state = replay_state(
        state, history_x, history_b, path_dt, conv_wx, conv_wb, accepted, dt_bias, a_rate, HPG
    )
    links, ancestry = tree_links(parents, keep)
    post_x = tree_conv(commit_rows(history_x, accepted, keep), x_rows, conv_wx, links, keep)
    post_b = tree_conv(commit_rows(history_b, accepted, keep), b_rows, conv_wb, links, keep)
    post_c = tree_conv(commit_rows(history_c, accepted, keep), c_rows, conv_wc, links, keep)
    gated = tree_mix(
        new_state,
        post_x,
        post_b,
        post_c,
        rate_rows,
        z_rows,
        ancestry,
        dt_bias,
        a_rate,
        d_skip,
        gain_out,
        HPG,
    )
    gated_flat = gated.reshape(-1, inner_local)
    summed = project_out(gated_flat, w_out, ranks, blocks)
    mixed = summed.reshape(seq_local, proposals, -1)
    return (mixed, new_state)


def solution(mesh):
    return jax.shard_map(
        shards,
        mesh=mesh,
        in_specs=(
            P(None, None, "kv"),
            P("kv", None),
            P("kv"),
            P("kv", "tp", None, None),
            P("kv", None, "tp"),
            P("kv", None, "tp"),
            P("kv", None, "tp"),
            P("kv", None, "tp"),
            P("kv", None, "tp"),
            P("kv", None, "tp"),
            P("kv", None, "tp"),
            P(),
            P("kv", "tp"),
            P("kv", "tp"),
            P("kv", "tp"),
            P("kv", "tp"),
            P(),
            P("tp"),
            P("tp"),
            P("tp"),
            P(None, "tp"),
            P(None, "tp"),
            P(None, "tp"),
            P("tp"),
            P("tp", "kv"),
        ),
        out_specs=(P("kv", None, "tp"), P("kv", "tp", None, None)),
        check_vma=False,
    )
```

profile of v0, /device:TPU:5, one launch (start us, length us, event | category | flops | bytes accessed | tf_op | source)
XLA Modules:
  0.0 194.5 jit_solution(11499063251229928607)
XLA Ops:
  1.4 1.3 dynamic_slice.6
  6.3 1.4 multiply_reduce_fusion
  7.6 0.8 fusion.104
  8.5 1.4 fusion.103
  10.9 0.9 fusion.9
  11.7 0.9 fusion.102
  15.6 0.8 copy.111
  19.2 1.0 copy.112
  21.3 0.9 broadcast_multiply_fusion
  23.6 1.3 reshape.176
  24.9 1.7 convolution_convert_fusion.1
  28.2 6.9 %convolution_convert_fusion = bf16[768,3072]{1,0:T(8,128)(2,1)} fusion(bf16[512,512]{1,0:T(8,128)(2,1)S(1)} %copy-done.35, bf16[512,512]{1,0:T(8,128)(2,1)} %param.39, bf16[512,1024]{1,0:T(8,128)(2,1)} %param.38, bf16[512,1024]{1,0:T(8,128)(2,1)} %param.37, f32[768,512]{1,0:T(8,128)} %reshape.176, f32[512]{0:T(512)S(1)} %copy-done.26), kind=kOutput, calls=%fused_computation | convolution fusion | flops 2431647744 | bytes 9439232 | tf_op jit(solution)/shard_map/dot_general | solution.py:573
  35.2 73.6 %shard_map.248 = (bf16[96,3072]{1,0:T(8,128)(2,1)}, bf16[96,128]{1,0:T(8,128)(2,1)}) custom-call(bf16[8,96,3072]{2,1,0:T(8,128)(2,1)} %bitcast.64, bf16[8,96,128]{2,1,0:T(8,128)(2,1)} %bitcast.70), custom_call_target="tpu_custom_call" | custom-call | tf_op jit(solution)/shard_map/pallas_call | solution.py:211
  111.4 1.0 fusion.100
  115.4 1.4 fusion.31
  120.4 1.2 broadcast_in_dim.26
  121.6 1.2 broadcast_in_dim.27
  122.8 2.7 %fusion.10 = f32[8,16,64,12]{2,3,1,0:T(8,128)S(1)} fusion(f32[8,12,16,64]{3,2,0,1:T(8,128)S(1)} %reshape.170, f32[8,16,12,12]{3,2,1,0:T(8,128)S(1)} %bitcast.65, f32[8,16,12]{2,1,0:T(8,128)} %copy.151, f32[8,16,12]{2,1,0:T(8,128)S(1)} %copy.149, pred[8,12,12]{2,1,0:T(8,128)(4,1)S(1)} %copy-done.9), kind=kOutput, calls=%fused_computation.20 | convolution fusion | flops 14247936 | bytes 873600 | tf_op jit(solution)/shard_map/shij,sjhp->sihp/dot_general | solution.py:518
  125.6 7.7 %multiply_add_fusion = f32[8,16,64,128]{3,2,1,0:T(8,128)S(1)} fusion(f32[8,16,64,128]{3,2,1,0:T(8,128)S(1)} %copy-done.2, f32[8,6,16,128]{3,1,2,0:T(8,128)S(1)} %bitcast.67, f32[8,16]{1,0:T(8,128)S(1)} %copy-done.24, f32[8,6,16,64]{3,2,0,1:T(8,128)S(1)} %copy-done.4), kind=kOutput, calls=%fused_computation.1 | convolution fusion | flops 77594624 | bytes 8978944 | tf_op jit(solution)/shard_map/sjh,sjhp,sjhn->shpn/dot_general | solution.py:453
  133.3 6.6 %fusion.106 = f32[8,16,64,12]{2,3,1,0:T(8,128)S(1)} fusion(f32[8,16,64,128]{3,2,1,0:T(8,128)S(1)} %multiply_add_fusion, f32[8,12,16,128]{3,1,2,0:T(8,128)S(1)} %bitcast.66), kind=kOutput, calls=%fused_computation.178 | convolution fusion | flops 150994944 | bytes 5373952 | tf_op jit(solution)/shard_map/sihn,shpn->sihp/dot_general | solution.py:508
  139.9 1.1 multiply_reduce_fusion.1
  141.8 1.7 multiply_convert_fusion.1.gated_ref
  143.6 49.2 %shard_map.249 = bf16[96,1024]{1,0:T(8,128)(2,1)} custom-call(bf16[96,1024]{1,0:T(8,128)(2,1)} %multiply_convert_fusion.1.gated_ref, bf16[1024,512]{1,0:T(8,128)(2,1)} %w_ref.1), custom_call_target="tpu_custom_call" | custom-call | tf_op jit(solution)/shard_map/pallas_call | solution.py:396
  192.7 1.0 reshape.175
  (159 shorter events, 25.2 us)
Async XLA Ops:
  0.6 24.2 %copy-start = (bf16[4096,64]{0,1:T(8,128)(2,1)S(1)}, bf16[4096,64]{0,1:T(8,128)(2,1)}, u32[]{:S(2)}) copy-start(bf16[4096,64]{0,1:T(8,128)(2,1)} %param.41) | copy-start | bytes 1572868
  1.4 11.3 %copy-start.31 = (f32[16]{0:T(128)}, f32[16]{0:T(128)S(1)}, u32[]{:S(2)}) copy-start(f32[16]{0:T(128)S(1)} %exponential_negate_fusion) | copy-start | bytes 196
  8.5 12.5 %copy-start.16 = (f32[1,512]{1,0:T(1,128)}, f32[1,512]{1,0:T(1,128)S(1)}, u32[]{:S(2)}) copy-start(f32[1,512]{1,0:T(1,128)S(1)} %get-tuple-element.30) | copy-start | bytes 6148
  8.5 12.5 %copy-start.18 = (f32[1,512]{1,0:T(1,128)}, f32[1,512]{1,0:T(1,128)S(1)}, u32[]{:S(2)}) copy-start(f32[1,512]{1,0:T(1,128)S(1)} %get-tuple-element.31) | copy-start | bytes 6148
  8.5 12.5 %copy-start.20 = (f32[1,512]{1,0:T(1,128)}, f32[1,512]{1,0:T(1,128)S(1)}, u32[]{:S(2)}) copy-start(f32[1,512]{1,0:T(1,128)S(1)} %get-tuple-element.32) | copy-start | bytes 6148
  8.5 12.5 %copy-start.22 = (f32[1,512]{1,0:T(1,128)}, f32[1,512]{1,0:T(1,128)S(1)}, u32[]{:S(2)}) copy-start(f32[1,512]{1,0:T(1,128)S(1)} %get-tuple-element.33) | copy-start | bytes 6148
  12.6 8.4 %copy-start.10 = (f32[1,1024]{1,0:T(1,128)}, f32[1,1024]{1,0:T(1,128)S(1)}, u32[]{:S(2)}) copy-start(f32[1,1024]{1,0:T(1,128)S(1)} %get-tuple-element.23) | copy-start | bytes 12292
  12.6 8.4 %copy-start.12 = (f32[1,1024]{1,0:T(1,128)}, f32[1,1024]{1,0:T(1,128)S(1)}, u32[]{:S(2)}) copy-start(f32[1,1024]{1,0:T(1,128)S(1)} %get-tuple-element.24) | copy-start | bytes 12292
  12.6 8.4 %copy-start.14 = (f32[1,1024]{1,0:T(1,128)}, f32[1,1024]{1,0:T(1,128)S(1)}, u32[]{:S(2)}) copy-start(f32[1,1024]{1,0:T(1,128)S(1)} %get-tuple-element.25) | copy-start | bytes 12292
  14.4 8.6 %copy-start.3 = (bf16[64,12,512]{2,0,1:T(8,128)(2,1)S(1)}, bf16[64,12,512]{2,0,1:T(8,128)(2,1)}, u32[]{:S(2)}) copy-start(bf16[64,12,512]{2,0,1:T(8,128)(2,1)} %param.25) | copy-start | bytes 2359300
  35.2 74.3 %copy-start.25 = (f32[16]{0:T(128)S(1)}, f32[16]{0:T(128)}, u32[]{:S(2)}) copy-start(f32[16]{0:T(128)} %param.42) | copy-start | bytes 196
  35.2 74.4 %copy-start.32 = (f32[16]{0:T(128)S(1)}, f32[16]{0:T(128)}, u32[]{:S(2)}) copy-start(f32[16]{0:T(128)} %copy-done.31) | copy-start | bytes 196
  35.2 77.3 %copy-start.8 = (bf16[8,3,512]{2,0,1:T(8,128)(2,1)S(1)}, bf16[8,3,512]{2,0,1:T(8,128)(2,1)}, u32[]{:S(2)}) copy-start(bf16[8,3,512]{2,0,1:T(8,128)(2,1)} %copy.265) | copy-start | bytes 73732
  109.6 4.9 %copy-start.17 = (f32[1,512]{1,0:T(1,128)S(1)}, f32[1,512]{1,0:T(1,128)}, u32[]{:S(2)}) copy-start(f32[1,512]{1,0:T(1,128)} %copy-done.16) | copy-start | bytes 6148
  109.6 4.9 %copy-start.19 = (f32[1,512]{1,0:T(1,128)S(1)}, f32[1,512]{1,0:T(1,128)}, u32[]{:S(2)}) copy-start(f32[1,512]{1,0:T(1,128)} %copy-done.18) | copy-start | bytes 6148
  109.6 4.9 %copy-start.21 = (f32[1,512]{1,0:T(1,128)S(1)}, f32[1,512]{1,0:T(1,128)}, u32[]{:S(2)}) copy-start(f32[1,512]{1,0:T(1,128)} %copy-done.20) | copy-start | bytes 6148
  109.6 4.9 %copy-start.23 = (f32[1,512]{1,0:T(1,128)S(1)}, f32[1,512]{1,0:T(1,128)}, u32[]{:S(2)}) copy-start(f32[1,512]{1,0:T(1,128)} %copy-done.22) | copy-start | bytes 6148
  120.0 5.6 %copy-start.4 = (f32[8,6,16,64]{3,2,0,1:T(8,128)S(1)}, f32[8,6,16,64]{3,2,0,1:T(8,128)}, u32[]{:S(2)}) copy-start(f32[8,6,16,64]{3,2,0,1:T(8,128)} %broadcast_multiply_fusion) | copy-start | bytes 589828
  120.0 5.6 %copy-start.5 = (f32[8,6,4,4,128]{4,1,3,2,0:T(8,128)S(1)}, f32[8,6,4,4,128]{4,1,3,2,0:T(8,128)}, u32[]{:S(2)}) copy-start(f32[8,6,4,4,128]{4,1,3,2,0:T(8,128)} %broadcast_in_dim.23) | copy-start | bytes 1179652
  120.0 5.6 %copy-start.24 = (f32[8,16]{1,0:T(8,128)S(1)}, f32[8,16]{1,0:T(8,128)}, u32[]{:S(2)}) copy-start(f32[8,16]{1,0:T(8,128)} %exp.57) | copy-start | bytes 1540
  120.4 5.1 %copy-start.2 = (f32[8,16,64,128]{3,2,1,0:T(8,128)S(1)}, f32[8,16,64,128]{3,2,1,0:T(8,128)}, u32[]{:S(2)}) copy-start(f32[8,16,64,128]{3,2,1,0:T(8,128)} %param.28) | copy-start | bytes 12582916
  133.3 7.8 %copy-start.1 = (f32[8,16,64,128]{3,2,1,0:T(8,128)}, f32[8,16,64,128]{3,2,1,0:T(8,128)S(1)}, u32[]{:S(2)}) copy-start(f32[8,16,64,128]{3,2,1,0:T(8,128)S(1)} %multiply_add_fusion) | copy-start | bytes 12582916
  133.3 6.6 %copy-start.7 = (f32[8,12,16]{2,1,0:T(8,128)S(1)}, f32[8,12,16]{2,1,0:T(8,128)}, u32[]{:S(2)}) copy-start(f32[8,12,16]{2,1,0:T(8,128)} %get-tuple-element.36) | copy-start | bytes 18436
  133.3 6.6 %copy-start.34 = (f32[16]{0:T(128)S(1)}, f32[16]{0:T(128)}, u32[]{:S(2)}) copy-start(f32[16]{0:T(128)} %param.44) | copy-start | bytes 196
  (12 other events, 43.8 us)
where the time goes:
time: 196 us; the launch traced here: 195 us
  Pallas kernels  123 us (63%)
  matrix products  32.9 us (17%)
  local copies, waits for them, and re-layouts  24.1 us (12%)
  other arithmetic  13.2 us (7%)
    pallas_call x1, Pallas kernels, scatter_rows(): pl.pallas_call(functools.partial(scatter_kernel, near, far, width, square...  73.6 us
    pallas_call x1, Pallas kernels, project_out(): pl.pallas_call(functools.partial(out_kernel, ranks, blocks), out_shape=ja...  49.2 us
    dot_general x1, matrix products, replay_state(): jnp.einsum('sjh,sjhp,sjhn->shpn', weights, path_xs, path_bh, precision=HIGH)  7.69 us
    dot_general x1, matrix products, shards(): jnp.dot(scaled, w_joined, preferred_element_type=jnp.float32)  6.94 us
    dot_general x1, matrix products, tree_mix(): jnp.einsum('sihn,shpn->sihp', c_heads, state, precision=HIGH)  6.62 us
    unnamed x81, local copies, waits for them, and re-layouts  6.16 us

commit v1 on v0

v1 whole, which is shorter than its diff:
```python
import functools

import jax
import jax.numpy as jnp
from jax import lax
from jax.experimental import pallas as pl
from jax.experimental.pallas import tpu as pltpu
from jax.sharding import PartitionSpec as P

HPG = 4
CORES = 2
EPS = 1e-06
HIGH = lax.Precision.HIGHEST
MESH = pl.DeviceIdType.MESH
F32 = jnp.float32
BF16 = jnp.bfloat16
LANES = 128


def inner_size(ranks):
    return max(d for d in range(1, ranks + 1) if ranks % d == 0 and d * d <= ranks)


def dot(a, b):
    return jnp.dot(a, b, preferred_element_type=F32)


def dot_nt(a, b):
    return lax.dot_general(a, b, (((1,), (1,)), ((), ())), preferred_element_type=F32)


def dot_high(a, b):
    return jnp.dot(a, b, precision=HIGH, preferred_element_type=F32)


def silu(x):
    return x * (1.0 / (1.0 + jnp.exp(-x)))


def softplus(x):
    return jnp.maximum(x, 0.0) + jnp.log1p(jnp.exp(-jnp.abs(x)))


def iota(shape, dim):
    return lax.broadcasted_iota(jnp.int32, shape, dim)


class Stream:
    def __init__(self, index, part, near, made, pair, onward, landed):
        self.index = index
        self.part, self.near, self.made = part, near, made
        self.pair, self.onward, self.landed = pair, onward, landed


def scatter_kernel(
    near,
    far,
    chunks,
    heads,
    width,
    tok_ref,
    gain_ref,
    wx_ref,
    wz_ref,
    wb_ref,
    wc_ref,
    wdt_ref,
    x_ref,
    z_ref,
    b_ref,
    c_ref,
    rate_ref,
    wbuf,
    wrate,
    scaled,
    part,
    near_in,
    made,
    pair_in,
    onward,
    far_in,
    side_part,
    side_near,
    side_made,
    side_pair,
    side_onward,
    side_far,
    zpart,
    zpair,
    zonward,
    zfar,
    zfin_out,
    zfin_in,
    w_sems,
    near_s,
    near_r,
    pair_s,
    pair_r,
    far_s,
    far_r,
    zpair_s,
    zpair_r,
    zfar_s,
    zfar_r,
    zfin_s,
    zfin_r,
):
    mine = lax.axis_index("kv")
    column = lax.axis_index("tp")
    my_far = mine // near
    my_near = lax.rem(mine, near)
    partner = my_far + 1 - 2 * lax.rem(my_far, 2)
    half = far // 2
    slab = scaled.shape[2]
    rows = scaled.shape[1]
    ranks = near * far
    wx_cols = wx_ref.shape[1] // chunks
    wb_cols = wb_ref.shape[1] // chunks
    first = 2 * wx_cols + wb_cols
    seqs = tok_ref.shape[1] // ranks

    loads = []
    for g in range(chunks):
        at = 0
        for k, (ref, cols) in enumerate(
            ((wx_ref, wx_cols), (wz_ref, wx_cols), (wb_ref, wb_cols), (wc_ref, wb_cols))
        ):
            copy = pltpu.make_async_copy(
                ref.at[:, pl.ds(g * cols, cols)], wbuf.at[g, :, pl.ds(at, cols)], w_sems.at[g, k]
            )
            copy.start()
            loads.append(copy)
            at += cols
    rate_load = pltpu.make_async_copy(
        wdt_ref.at[
            pl.ds(pl.multiple_of(column * heads, heads), heads),
            pl.ds(pl.multiple_of(mine * slab, slab), slab),
        ],
        wrate,
        w_sems.at[chunks, 0],
    )
    rate_load.start()

    def place(home, jump, step_near):
        return lax.rem(home + 2 * jump, far) * near + lax.rem(my_near + step_near, near)

    barrier = pltpu.get_barrier_semaphore()
    peers = [place(my_far, 0, step) for step in range(1, near)]
    peers = peers + [place(partner, 0, 0)]
    peers = peers + [place(my_far, jump, 0) for jump in range(1, half)]
    for peer in peers:
        pl.semaphore_signal(barrier, inc=1, device_id=(peer, column), device_id_type=MESH)

    rate_load.wait()
    gain = gain_ref[:, pl.ds(pl.multiple_of(mine * slab, slab), slab)]
    rate_w = wrate[...]

    @pl.loop(0, ranks)
    def _(d):
        tokens = tok_ref[:, pl.ds(pl.multiple_of(d * seqs, seqs), seqs), :].astype(F32).reshape(rows, slab)
        block = (tokens * gain).astype(BF16)
        scaled[d] = block
        squares = jnp.sum(tokens * tokens, axis=1, keepdims=True)
        rates = dot_nt(block, rate_w)
        side_part[d, :, 0:heads] = rates.astype(BF16)
        side_part[d, :, heads : heads + 1] = squares.astype(BF16)

    def multiply(g):
        for copy in loads[4 * g : 4 * g + 4]:
            copy.wait()

        @pl.loop(0, ranks // 2)
        def _(turn):
            block = scaled[pl.ds(2 * turn, 2)].reshape(2 * rows, slab)
            both = dot(block, wbuf[g]).astype(BF16)
            for k in range(2):
                part[g, 2 * turn + k] = both[k * rows : (k + 1) * rows, :first]
                zpart[g, 2 * turn + k] = both[k * rows : (k + 1) * rows, first:]

    order = [(jump, kind) for jump in list(range(1, half)) + [0] for kind in range(2)]
    turns = len(order)
    homes = (partner, my_far)
    side = Stream(chunks, side_part, side_near, side_made, side_pair, side_onward, side_far)
    streams = []
    for g in range(chunks):
        stream = Stream(
            g, part.at[g], near_in.at[g], made.at[g], pair_in.at[g], onward.at[g], far_in.at[g]
        )
        streams.append([side, stream] if g == 0 else [stream])

    copies = []
    waits = {}

    def send(key, source, landing, send_sem, recv_sem, target):
        copy = pltpu.make_async_remote_copy(
            src_ref=source,
            dst_ref=landing,
            send_sem=send_sem,
            recv_sem=recv_sem,
            device_id=(target, column),
            device_id_type=MESH,
        )
        copy.start()
        copies.append(copy)
        waits[key] = copy

    def start_near(q):
        g, t = q // turns, q % turns
        jump, kind = order[t]
        slot = 2 * jump + kind
        for step in range(1, near):
            for s in streams[g]:
                send(
                    ("near", s.index, slot, step),
                    s.part.at[place(homes[kind], jump, step)],
                    s.near.at[slot, step - 1],
                    near_s.at[s.index, slot, step - 1],
                    near_r.at[s.index, slot, step - 1],
                    place(my_far, 0, step),
                )

    def start_zpair(g):
        for jump in list(range(1, half)) + [0]:
            for step in range(near):
                send(
                    ("zpair", g, jump, step),
                    zpart.at[g, place(partner, jump, step)],
                    zpair.at[g, jump, step],
                    zpair_s.at[g, jump, step],
                    zpair_r.at[g, jump, step],
                    place(partner, 0, 0),
                )

    def sum_of(first_term, others):
        total = first_term.astype(F32)
        for other in others:
            total = total + other.astype(F32)
        return total

    def near_terms(s, slot):
        return [s.near[slot, step - 1] for step in range(1, near)]

    def step_kind0(g, jump):
        slot = 2 * jump
        for s in streams[g]:
            for step in range(1, near):
                waits["near", s.index, slot, step].wait_recv()
            s.made[jump] = sum_of(s.part[place(partner, jump, 0)], near_terms(s, slot)).astype(BF16)
            send(
                ("pair", s.index, jump),
                s.made.at[jump],
                s.pair.at[jump],
                pair_s.at[s.index, jump],
                pair_r.at[s.index, jump],
                place(partner, 0, 0),
            )

    def step_kind1(g, jump):
        slot = 2 * jump + 1
        for s in streams[g]:
            for step in range(1, near):
                waits["near", s.index, slot, step].wait_recv()
            if jump == 0:
                continue
            waits["pair", s.index, jump].wait_recv()
            s.onward[jump - 1] = sum_of(
                s.part[place(my_far, jump, 0)], near_terms(s, slot) + [s.pair[jump]]
            ).astype(BF16)
            send(
                ("far", s.index, jump),
                s.onward.at[jump - 1],
                s.landed.at[jump - 1],
                far_s.at[s.index, jump - 1],
                far_r.at[s.index, jump - 1],
                place(my_far, jump, 0),
            )

    def z_onward(g):
        for jump in range(1, half):
            for step in range(near):
                waits["zpair", g, jump, step].wait_recv()
                zonward[g, jump - 1, step] = sum_of(
                    zpart[g, place(my_far, jump, step)], [zpair[g, jump, step]]
                ).astype(BF16)
                send(
                    ("zfar", g, jump, step),
                    zonward.at[g, jump - 1, step],
                    zfar.at[g, jump - 1, step],
                    zfar_s.at[g, jump - 1, step],
                    zfar_r.at[g, jump - 1, step],
                    place(my_far, jump, 0),
                )

    def z_terms(g, step):
        return [zpair[g, 0, step]] + [zfar[g, jump - 1, step] for jump in range(1, half)]

    def z_last(g):
        for step in range(near):
            waits["zpair", g, 0, step].wait_recv()
            for jump in range(1, half):
                waits["zfar", g, jump, step].wait_recv()
        for step in range(1, near):
            zfin_out[g, step - 1] = sum_of(
                zpart[g, place(my_far, 0, step)], z_terms(g, step)
            ).astype(BF16)
            send(
                ("zfin", g, step),
                zfin_out.at[g, step - 1],
                zfin_in.at[g, step - 1],
                zfin_s.at[g, step - 1],
                zfin_r.at[g, step - 1],
                place(my_far, 0, step),
            )

    scale = []

    def finish(g):
        for s in streams[g]:
            waits["pair", s.index, 0].wait_recv()
            for jump in range(1, half):
                waits["far", s.index, jump].wait_recv()
            total = sum_of(
                s.part[mine],
                near_terms(s, 1) + [s.pair[0]] + [s.landed[jump - 1] for jump in range(1, half)],
            )
            if s is side:
                scale.append(lax.rsqrt(total[:, heads : heads + 1] / width + EPS))
                rate_ref[...] = (total[:, 0:heads] * scale[0]).astype(BF16)
            else:
                total = (total * scale[0]).astype(BF16)
                x_ref[:, g * wx_cols : (g + 1) * wx_cols] = total[:, :wx_cols]
                z_ref[:, g * wx_cols : (g + 1) * wx_cols] = total[:, wx_cols : 2 * wx_cols]
                b_ref[:, g * wb_cols : (g + 1) * wb_cols] = total[:, 2 * wx_cols :]
        for step in range(1, near):
            waits["zfin", g, step].wait_recv()
        total = sum_of(
            zpart[g, mine], z_terms(g, 0) + [zfin_in[g, step - 1] for step in range(1, near)]
        )
        c_ref[:, g * wb_cols : (g + 1) * wb_cols] = (total * scale[0]).astype(BF16)

    ahead = 3
    multiply(0)
    pl.semaphore_wait(barrier, len(peers))
    for q in range(min(ahead, chunks * turns)):
        if q > 0 and q % turns == 0:
            multiply(q // turns)
        start_near(q)
    start_zpair(0)
    for g in range(chunks):
        if g + 1 < chunks and turns > ahead:
            multiply(g + 1)
        for t, (jump, kind) in enumerate(order):
            if kind == 0:
                step_kind0(g, jump)
            else:
                step_kind1(g, jump)
            if g * turns + t + ahead < chunks * turns:
                start_near(g * turns + t + ahead)
            if t == 0:
                z_onward(g)
            if t == 1 and g + 1 < chunks:
                start_zpair(g + 1)
            if t == turns - 2:
                z_last(g)
        if g > 0:
            finish(g - 1)
    finish(chunks - 1)
    for copy in copies:
        copy.wait_send()


def scatter_rows(tokens, gain, w_x, w_z, w_b, w_c, w_dt, heads, ranks, chunks):
    props, all_seqs, slab = tokens.shape
    rows = props * all_seqs // ranks
    near = inner_size(ranks)
    far = ranks // near
    half = far // 2
    xc = w_x.shape[1] // chunks
    bc = w_b.shape[1] // chunks
    wide = 2 * xc + bc
    vmem = pl.BlockSpec(memory_space=pltpu.VMEM)
    hbm = pl.BlockSpec(memory_space=pl.ANY)
    dma = pltpu.SemaphoreType.DMA

    def buf(*shape):
        return pltpu.VMEM(shape, BF16)

    scratch = [
        buf(chunks, slab, wide + bc),
        buf(heads, slab),
        buf(ranks, rows, slab),
        buf(chunks, ranks, rows, wide),
        buf(chunks, far, near - 1, rows, wide),
        buf(chunks, half, rows, wide),
        buf(chunks, half, rows, wide),
        buf(chunks, half - 1, rows, wide),
        buf(chunks, half - 1, rows, wide),
        buf(ranks, rows, LANES),
        buf(far, near - 1, rows, LANES),
        buf(half, rows, LANES),
        buf(half, rows, LANES),
        buf(half - 1, rows, LANES),
        buf(half - 1, rows, LANES),
        buf(chunks, ranks, rows, bc),
        buf(chunks, half, near, rows, bc),
        buf(chunks, half - 1, near, rows, bc),
        buf(chunks, half - 1, near, rows, bc),
        buf(chunks, near - 1, rows, bc),
        buf(chunks, near - 1, rows, bc),
        dma((chunks + 1, 4)),
    ]
    for shape in (
        (chunks + 1, far, near - 1),
        (chunks + 1, half),
        (chunks + 1, half - 1),
        (chunks, half, near),
        (chunks, half - 1, near),
        (chunks, near - 1),
    ):
        scratch += [dma(shape), dma(shape)]
    return pl.pallas_call(
        functools.partial(scatter_kernel, near, far, chunks, heads, gain.shape[1]),
        out_shape=(
            jax.ShapeDtypeStruct((rows, w_x.shape[1]), BF16),
            jax.ShapeDtypeStruct((rows, w_z.shape[1]), BF16),
            jax.ShapeDtypeStruct((rows, w_b.shape[1]), BF16),
            jax.ShapeDtypeStruct((rows, w_c.shape[1]), BF16),
            jax.ShapeDtypeStruct((rows, heads), BF16),
        ),
        in_specs=[vmem, vmem, hbm, hbm, hbm, hbm, hbm],
        out_specs=(vmem,) * 5,
        scratch_shapes=scratch,
        compiler_params=pltpu.CompilerParams(collective_id=0, has_side_effects=True),
        name="scatter",
    )(tokens, gain, w_x, w_z, w_b, w_c, w_dt)


def spread(values, g, lanes):
    head = lanes // HPG
    lane = iota((1, lanes), 1)
    out = values[:, HPG * g : HPG * g + 1]
    for i in range(1, HPG):
        out = jnp.where(lane >= i * head, values[:, HPG * g + i : HPG * g + i + 1], out)
    return out


def mix_kernel(
    x_ref,
    z_ref,
    b_ref,
    c_ref,
    rate_ref,
    parents_ref,
    accepted_ref,
    state_ref,
    conv_x_ref,
    conv_b_ref,
    conv_c_ref,
    path_x_ref,
    path_b_ref,
    path_c_ref,
    path_dt_ref,
    bias_ref,
    alog_ref,
    skip_ref,
    wx_ref,
    wb_ref,
    wc_ref,
    gain_ref,
    gated_ref,
    new_ref,
    hist,
    state_vm,
    new_vm,
    new_bf,
    in_sems,
    out_sems,
):
    seqs, heads, head_dim, state_dim = state_ref.shape
    groups = heads // HPG
    props = parents_ref.shape[1]
    rows = seqs * props
    keep, path_len = conv_x_ref.shape[0], path_x_ref.shape[0]
    taps = keep + 1
    held = keep + path_len
    hrows, prows = held * seqs, path_len * seqs
    xc, bc = HPG * head_dim, state_dim
    wide = xc + 2 * bc
    low = seqs - 1
    shift = seqs.bit_length() - 1

    loads = []
    for g in range(groups):
        copy = pltpu.make_async_copy(
            state_ref.at[:, pl.ds(HPG * g, HPG)], state_vm.at[g], in_sems.at[g]
        )
        copy.start()
        loads.append(copy)

    for g in range(groups):
        at = 0
        for conv, path, cols in (
            (conv_x_ref, path_x_ref, xc),
            (conv_b_ref, path_b_ref, bc),
            (conv_c_ref, path_c_ref, bc),
        ):
            span = slice(g * cols, (g + 1) * cols)
            top = conv[:, :, span].astype(F32).reshape(keep * seqs, cols)
            end = path[:, :, span].astype(F32).reshape(prows, cols)
            hist[g, :, at : at + cols] = jnp.concatenate([top, end], axis=0).astype(BF16)
            at += cols

    def tap(k, g, parts):
        refs = ((wx_ref, xc), (wb_ref, bc), (wc_ref, bc))
        return jnp.concatenate(
            [ref[k : k + 1, g * cols : (g + 1) * cols].astype(F32) for ref, cols in refs[:parts]],
            axis=1,
        )

    bias = bias_ref[...]
    a_rate = -jnp.exp(alog_ref[...])
    eye = iota((seqs, seqs), 0) == iota((seqs, seqs), 1)
    accepted = jnp.sum(
        jnp.where(eye, accepted_ref[...].astype(F32), 0.0), axis=1, keepdims=True
    )

    acc_path = jnp.concatenate([accepted] * path_len, axis=0)
    step_of = lax.shift_right_logical(iota((prows, 1), 0), shift).astype(F32)
    live = (step_of < acc_path).astype(F32)
    path_step = softplus(path_dt_ref[...].astype(F32).reshape(prows, heads) + bias)
    log_decay = path_step * a_rate * live
    pr, pc = iota((prows, prows), 0), iota((prows, prows), 1)
    same = (pr & low) == (pc & low)
    later = jnp.where(same & (pc > pr), 1.0, 0.0)
    tail = dot_high(later, log_decay)
    every = jnp.where(iota((seqs, prows), 0) == (iota((seqs, prows), 1) & low), 1.0, 0.0)
    overall = jnp.exp(dot_high(every, log_decay))
    weights = live * jnp.exp(tail) * path_step
    block_mask = (iota((prows, seqs * bc), 0) & low) == lax.shift_right_logical(
        iota((prows, seqs * bc), 1), bc.bit_length() - 1
    )

    for g in range(groups):
        values = hist[g, :, 0 : xc + bc].astype(F32)
        summed = tap(0, g, 2) * values[0:prows]
        for k in range(1, taps):
            summed = summed + tap(k, g, 2) * values[k * seqs : k * seqs + prows]
        post = silu(summed)
        left = (post[:, :xc] * spread(weights, g, xc)).T.astype(BF16)
        right = jnp.where(block_mask, jnp.concatenate([post[:, xc:]] * seqs, axis=1), 0.0)
        grown = dot(left, right.astype(BF16))
        loads[g].wait()
        for s in range(seqs):
            for i in range(HPG):
                h = HPG * g + i
                fresh = (
                    overall[s : s + 1, h : h + 1] * state_vm[g, s, i]
                    + grown[i * head_dim : (i + 1) * head_dim, s * bc : (s + 1) * bc]
                )
                new_vm[g, s, i] = fresh
                new_bf[g, i * head_dim : (i + 1) * head_dim, s * bc : (s + 1) * bc] = fresh.astype(
                    BF16
                )
        pltpu.make_async_copy(
            new_vm.at[g], new_ref.at[:, pl.ds(HPG * g, HPG)], out_sems.at[g]
        ).start()

    parents = parents_ref[...].astype(F32)
    parent = jnp.concatenate([parents[:, i : i + 1] for i in range(props)], axis=0)
    acc_rows = jnp.concatenate([accepted] * props, axis=0)
    seq_of = (iota((rows, 1), 0) & low).astype(F32)
    in_tree = parent >= 0.0
    hist_at = jnp.where(in_tree, -1.0, (acc_rows + (keep - 1)) * seqs + seq_of)
    prop_at = jnp.where(in_tree, parent * seqs + seq_of, -1.0)
    link_p = iota((rows, rows), 1).astype(F32) == prop_at
    link_h = iota((rows, hrows), 1).astype(F32) == hist_at
    up_p = jnp.where(link_p, 1.0, 0.0).astype(BF16)
    up_h = jnp.where(link_h, 1.0, 0.0).astype(BF16)
    back = jnp.where(
        iota((hrows, hrows), 1) == iota((hrows, hrows), 0) - seqs, 1.0, 0.0
    ).astype(BF16)
    ups_p, ups_h = [up_p], [up_h]
    for _ in range(1, taps - 1):
        last_p, last_h = ups_p[-1], ups_h[-1]
        ups_p.append(dot(last_p, up_p).astype(BF16))
        ups_h.append((dot(last_p, up_h) + dot(last_h, back)).astype(BF16))
    all_p = jnp.concatenate(ups_p, axis=0)
    all_h = jnp.concatenate(ups_h, axis=0)
    self_at = iota((rows, rows), 0) == iota((rows, rows), 1)
    tree = jnp.where(link_p | self_at, 1.0, 0.0)
    for _ in range((props - 1).bit_length()):
        some = tree.astype(BF16)
        tree = jnp.minimum(dot(some, some), 1.0)
    above = tree > 0.5

    step_size = softplus(rate_ref[...].astype(F32) + bias)
    decay = dot_high(tree, step_size * a_rate)
    decay_t = decay.T
    step_t = step_size.T
    carried_scale = jnp.exp(decay)
    own = (iota((rows, seqs * bc), 0) & low) == lax.shift_right_logical(
        iota((rows, seqs * bc), 1), bc.bit_length() - 1
    )
    lane = iota((1, xc), 1)

    for g in range(groups):
        here = jnp.concatenate(
            [
                x_ref[:, g * xc : (g + 1) * xc],
                b_ref[:, g * bc : (g + 1) * bc],
                c_ref[:, g * bc : (g + 1) * bc],
            ],
            axis=1,
        )
        summed = tap(taps - 1, g, 3) * here.astype(F32)
        reached = dot(all_p, here) + dot(all_h, hist[g])
        for k in range(1, taps):
            summed = summed + tap(taps - 1 - k, g, 3) * reached[(k - 1) * rows : k * rows]
        post = silu(summed)
        post_x = post[:, :xc]
        post_b = post[:, xc : xc + bc].astype(BF16)
        post_c = post[:, xc + bc :]
        scores = dot_nt(post_c.astype(BF16), post_b)
        out = jnp.zeros((rows, xc), F32)
        for i in range(HPG):
            h = HPG * g + i
            gap = decay[:, h : h + 1] - decay_t[h : h + 1, :]
            mixing = jnp.where(above, jnp.exp(jnp.where(above, gap, 0.0)), 0.0)
            mixing = scores * mixing * step_t[h : h + 1, :]
            mine = (lane >= i * head_dim) & (lane < (i + 1) * head_dim)
            out = out + dot(mixing.astype(BF16), jnp.where(mine, post_x, 0.0).astype(BF16))
        wide_c = jnp.where(own, jnp.concatenate([post_c] * seqs, axis=1), 0.0).astype(BF16)
        carried = dot_nt(wide_c, new_bf[g])
        out = out + carried * spread(carried_scale, g, xc) + spread(skip_ref[...], g, xc) * post_x
        out = out * silu(z_ref[:, g * xc : (g + 1) * xc].astype(F32))
        out = out * lax.rsqrt(jnp.mean(out * out, axis=1, keepdims=True) + EPS)
        gated_ref[:, g * xc : (g + 1) * xc] = (out * gain_ref[:, g * xc : (g + 1) * xc]).astype(
            BF16
        )
    for g in range(groups):
        pltpu.make_async_copy(
            new_vm.at[g], new_ref.at[:, pl.ds(HPG * g, HPG)], out_sems.at[g]
        ).wait()


def mix(projected, parents, accepted, state, conv, path, path_dt, small, taps, gain_out):
    rows, inner = projected[0].shape
    seqs, heads, head_dim, state_dim = state.shape
    groups = heads // HPG
    held = conv[0].shape[0] + path[0].shape[0]
    vmem = pl.BlockSpec(memory_space=pltpu.VMEM)
    hbm = pl.BlockSpec(memory_space=pl.ANY)
    return pl.pallas_call(
        mix_kernel,
        out_shape=(
            jax.ShapeDtypeStruct((rows, inner), BF16),
            jax.ShapeDtypeStruct(state.shape, F32),
        ),
        in_specs=[vmem] * 7 + [hbm] + [vmem] * 14,
        out_specs=(vmem, hbm),
        scratch_shapes=[
            pltpu.VMEM((groups, held * seqs, HPG * head_dim + 2 * state_dim), BF16),
            pltpu.VMEM((groups, seqs, HPG, head_dim, state_dim), F32),
            pltpu.VMEM((groups, seqs, HPG, head_dim, state_dim), F32),
            pltpu.VMEM((groups, HPG * head_dim, seqs * state_dim), BF16),
            pltpu.SemaphoreType.DMA((groups,)),
            pltpu.SemaphoreType.DMA((groups,)),
        ],
        name="mix",
    )(*projected, parents, accepted, state, *conv, *path, path_dt, *small, *taps, gain_out)


def out_kernel(
    near,
    far,
    ratio,
    cores,
    gated_ref,
    w_ref,
    mixed_ref,
    w_vm,
    gathered,
    terms,
    sibling_in,
    paired,
    column_in,
    done,
    landed,
    w_sem,
    gather_s,
    gather_r,
    sib_s,
    sib_r,
    col_s,
    col_r,
    done_s,
    done_r,
):
    mine = lax.axis_index("kv")
    column = lax.axis_index("tp")
    blocks = lax.axis_size("tp")
    ranks = near * far
    half = far // 2
    depth = blocks // cores
    my_far = mine // near
    my_near = lax.rem(mine, near)
    partner = my_far + 1 - 2 * lax.rem(my_far, 2)
    core = lax.rem(column, cores)
    level = column // cores
    owner = mine // ratio
    spot = lax.rem(mine, ratio)
    owner_level = owner // cores
    owner_core = lax.rem(owner, cores)
    slab = w_ref.shape[1]

    load = pltpu.make_async_copy(w_ref, w_vm, w_sem)
    load.start()

    def place(home, jump, step_near):
        return lax.rem(home + 2 * jump, far) * near + lax.rem(my_near + step_near, near)

    barrier = pltpu.get_barrier_semaphore()

    def greet(target):
        pl.semaphore_signal(barrier, inc=1, device_id=target, device_id_type=MESH)

    count = 0
    for peer in (
        [place(my_far, jump, 0) for jump in range(1, half)]
        + [place(partner, 0, 0)]
        + [place(my_far, 0, step) for step in range(1, near)]
    ):
        greet((peer, column))
        count += 1
    for other in range(1, cores):
        greet((mine, level * cores + lax.rem(core + other, cores)))
        count += 1

    @pl.when(level != owner_level)
    def _():
        greet((mine, owner_level * cores + core))

    for up in range(1, depth):

        @pl.when(level == owner_level)
        def _():
            greet((mine, lax.rem(level + up, depth) * cores + core))

    for n in range(ratio):
        for c in range(cores):
            source = column * ratio + n

            @pl.when(jnp.logical_or(source != mine, c != core))
            def _():
                greet((source, level * cores + c))

    @pl.when(level != owner_level)
    def _():
        pl.semaphore_wait(barrier, count + 1)

    @pl.when(jnp.logical_and(level == owner_level, core != owner_core))
    def _():
        pl.semaphore_wait(barrier, count + depth - 1 + ranks)

    @pl.when(jnp.logical_and(level == owner_level, core == owner_core))
    def _():
        pl.semaphore_wait(barrier, count + depth - 1 + ranks - 1)

    index = {}
    for home in range(2):
        for jump in range(half):
            for step in range(near):
                index[jump, home, step] = len(index)
    homes = (my_far, partner)

    def origin(key):
        jump, home, step = key
        return lax.rem(homes[home] + 2 * (half - jump) % far, far) * near + lax.rem(
            my_near + near - step, near
        )

    copies = []
    waits = {}

    def gather(key, source, target):
        k = index[key]
        copy = pltpu.make_async_remote_copy(
            src_ref=source,
            dst_ref=gathered.at[k],
            send_sem=gather_s.at[k],
            recv_sem=gather_r.at[k],
            device_id=(target, column),
            device_id_type=MESH,
        )
        copy.start()
        copies.append(copy)
        waits[key] = copy

    def block_ref(key):
        return gated_ref if key == (0, 0, 0) else gathered.at[index[key]]

    for jump in range(1, half):
        gather((jump, 0, 0), gated_ref, place(my_far, jump, 0))
    gather((0, 1, 0), gated_ref, place(partner, 0, 0))
    for step in range(1, near):
        gather((0, 0, step), gated_ref, place(my_far, 0, step))
    load.wait()

    def multiply(key):
        if key != (0, 0, 0):
            waits[key].wait_recv()
        jump, home, step = key
        if home == 0 and jump > 0 and step == 0:
            gather((jump, 1, 0), block_ref(key), place(partner, 0, 0))
        if step == 0 and (home, jump) != (0, 0):
            for s in range(1, near):
                gather((jump, home, s), block_ref(key), place(my_far, 0, s))
        terms[index[key]] = dot(block_ref(key)[...], w_vm[...]).astype(BF16)

    order = [(0, 0, 0)] + [(jump, 0, 0) for jump in range(1, half)]
    order += [(0, 1, 0)] + [(0, 0, step) for step in range(1, near)]
    order += [(jump, 1, 0) for jump in range(1, half)]
    order += [(jump, 0, step) for jump in range(1, half) for step in range(1, near)]
    order += [(jump, 1, step) for jump in range(half) for step in range(1, near)]
    batches = [order[at : at + cores] for at in range(0, len(order), cores)]

    def pick(keys, which):
        out = index[keys[0]]
        for k in range(1, cores):
            out = jnp.where(which == k, index[keys[k]], out)
        return out

    def pick_origin(keys, which):
        out = origin(keys[0])
        for k in range(1, cores):
            out = jnp.where(which == k, origin(keys[k]), out)
        return out

    def sibling_copy(n, other):
        target = lax.rem(core + other, cores)
        return pltpu.make_async_remote_copy(
            src_ref=terms.at[pick(batches[n], target)],
            dst_ref=sibling_in.at[n, other - 1],
            send_sem=sib_s.at[n, other - 1],
            recv_sem=sib_r.at[n, other - 1],
            device_id=(mine, level * cores + target),
            device_id_type=MESH,
        )

    def column_copy(n, up):
        return pltpu.make_async_remote_copy(
            src_ref=paired.at[n],
            dst_ref=column_in.at[n, up - 1],
            send_sem=col_s.at[n],
            recv_sem=col_r.at[n, up - 1],
            device_id=(mine, owner_level * cores + core),
            device_id_type=MESH,
        )

    def done_copy(n):
        return pltpu.make_async_remote_copy(
            src_ref=done.at[n],
            dst_ref=landed.at[spot],
            send_sem=done_s.at[n],
            recv_sem=done_r.at[spot],
            device_id=(pick_origin(batches[n], core), owner),
            device_id_type=MESH,
        )

    def stays(n):
        if (0, 0, 0) not in batches[n]:
            return None
        return jnp.logical_and(core == batches[n].index((0, 0, 0)), owner == column)

    def level_gap():
        return lax.rem(level - owner_level + depth, depth)

    def pair_up(n):
        total = terms[pick(batches[n], core)].astype(F32)
        for other in range(1, cores):
            sibling_copy(n, other).wait_recv()
            total = total + sibling_in[n, other - 1].astype(F32)
        paired[n] = total.astype(BF16)
        for up in range(1, depth):

            @pl.when(level_gap() == up)
            def _():
                column_copy(n, up).start()

    def finish(n):
        @pl.when(level == owner_level)
        def _():
            total = paired[n].astype(F32)
            for up in range(1, depth):
                column_copy(n, up).wait_recv()
                total = total + column_in[n, up - 1].astype(F32)
            done[n] = total.astype(BF16)
            here = stays(n)
            if here is None:
                done_copy(n).start()
            else:

                @pl.when(here)
                def _():
                    landed[spot] = done[n]

                @pl.when(jnp.logical_not(here))
                def _():
                    done_copy(n).start()

    for n, keys in enumerate(batches):
        for key in keys:
            multiply(key)
        for other in range(1, cores):
            sibling_copy(n, other).start()
        if n >= 1:
            pair_up(n - 1)
        if n >= 2:
            finish(n - 2)
    last = len(batches) - 1
    pair_up(last)
    if last >= 1:
        finish(last - 1)
    finish(last)

    for n in range(ratio):
        source = column * ratio + n
        local = jnp.logical_and(source == mine, core == batches[0].index((0, 0, 0)))

        @pl.when(jnp.logical_not(local))
        def _():
            pltpu.make_async_remote_copy(
                src_ref=done.at[0],
                dst_ref=landed.at[n],
                send_sem=done_s.at[0],
                recv_sem=done_r.at[n],
                device_id=(source, lax.rem(column + 1, blocks)),
                device_id_type=MESH,
            ).wait_recv()

        mixed_ref[:, n * slab : (n + 1) * slab] = landed[n]

    for copy in copies:
        copy.wait_send()
    for n in range(len(batches)):
        for other in range(1, cores):
            sibling_copy(n, other).wait_send()

        @pl.when(level != owner_level)
        def _():
            column_copy(n, 1).wait_send()

        @pl.when(level == owner_level)
        def _():
            here = stays(n)
            if here is None:
                done_copy(n).wait_send()
            else:

                @pl.when(jnp.logical_not(here))
                def _():
                    done_copy(n).wait_send()


def project_out(gated, w_out, ranks, blocks):
    rows = gated.shape[0]
    inner, slab = w_out.shape
    near = inner_size(ranks)
    far = ranks // near
    ratio = ranks // blocks
    depth = blocks // CORES
    batches = ranks // CORES
    vmem = pl.BlockSpec(memory_space=pltpu.VMEM)
    hbm = pl.BlockSpec(memory_space=pl.ANY)
    dma = pltpu.SemaphoreType.DMA
    return pl.pallas_call(
        functools.partial(out_kernel, near, far, ratio, CORES),
        out_shape=jax.ShapeDtypeStruct((rows, ratio * slab), BF16),
        in_specs=[vmem, hbm],
        out_specs=vmem,
        scratch_shapes=[
            pltpu.VMEM((inner, slab), BF16),
            pltpu.VMEM((ranks, rows, inner), BF16),
            pltpu.VMEM((ranks, rows, slab), BF16),
            pltpu.VMEM((batches, CORES - 1, rows, slab), BF16),
            pltpu.VMEM((batches, rows, slab), BF16),
            pltpu.VMEM((batches, depth - 1, rows, slab), BF16),
            pltpu.VMEM((batches, rows, slab), BF16),
            pltpu.VMEM((ratio, rows, slab), BF16),
            dma(()),
            dma((ranks,)),
            dma((ranks,)),
            dma((batches, CORES - 1)),
            dma((batches, CORES - 1)),
            dma((batches,)),
            dma((batches, depth - 1)),
            dma((batches,)),
            dma((ratio,)),
        ],
        compiler_params=pltpu.CompilerParams(collective_id=1, has_side_effects=True),
        name="project_out",
    )(gated, w_out)


def shards(
    tokens,
    parents,
    accepted,
    state,
    conv_x,
    conv_b,
    conv_c,
    path_x,
    path_b,
    path_c,
    path_dt,
    gain_in,
    w_x,
    w_z,
    w_b,
    w_c,
    w_dt,
    dt_bias,
    a_log,
    d_skip,
    conv_wx,
    conv_wb,
    conv_wc,
    gain_out,
    w_out,
):
    ranks = lax.axis_size("kv")
    blocks = lax.axis_size("tp")
    heads = dt_bias.shape[0]

    def front(array):
        return jnp.swapaxes(array, 0, 1)

    projected = scatter_rows(
        front(tokens),
        gain_in[None, :],
        w_x,
        w_z,
        w_b,
        w_c,
        w_dt.T,
        heads,
        ranks,
        heads // HPG,
    )
    gated, new_state = mix(
        projected,
        parents,
        accepted[None, :],
        state,
        (front(conv_x), front(conv_b), front(conv_c)),
        (front(path_x), front(path_b), front(path_c)),
        front(path_dt),
        (dt_bias[None, :], a_log[None, :], d_skip[None, :]),
        (conv_wx, conv_wb, conv_wc),
        gain_out[None, :],
    )
    summed = project_out(gated, w_out, ranks, blocks)
    seqs, props = parents.shape
    mixed = front(summed.reshape(props, seqs, summed.shape[1]))
    return (mixed, new_state)


def solution(mesh):
    return jax.shard_map(
        shards,
        mesh=mesh,
        in_specs=(
            P(None, None, "kv"),
            P("kv", None),
            P("kv"),
            P("kv", "tp", None, None),
            P("kv", None, "tp"),
            P("kv", None, "tp"),
            P("kv", None, "tp"),
            P("kv", None, "tp"),
            P("kv", None, "tp"),
            P("kv", None, "tp"),
            P("kv", None, "tp"),
            P(),
            P("kv", "tp"),
            P("kv", "tp"),
            P("kv", "tp"),
            P("kv", "tp"),
            P(),
            P("tp"),
            P("tp"),
            P("tp"),
            P(None, "tp"),
            P(None, "tp"),
            P(None, "tp"),
            P("tp"),
            P("tp", "kv"),
        ),
        out_specs=(P("kv", None, "tp"), P("kv", "tp", None, None)),
        check_vma=False,
    )
```

time: 196 us -> 112 us (0.57)
  the two profiles are of different devices: /device:TPU:5 before, /device:TPU:0 now
where the time goes in v1:
time: 112 us
  Pallas kernels  109 us (97%)
  local copies, waits for them, and re-layouts  1.62 us (1%)
    pallas_call x1, Pallas kernels, scatter_rows(): pl.pallas_call(functools.partial(scatter_kernel, near, far, chunks, heads...  63.1 us
    pallas_call x1, Pallas kernels, project_out(): pl.pallas_call(functools.partial(out_kernel, near, far, ratio, CORES), ou...  37.1 us
    pallas_call x1, Pallas kernels, mix(): pl.pallas_call(mix_kernel, out_shape=(jax.ShapeDtypeStruct((rows, inner),...  9.29 us

profile of v1, /device:TPU:0, one launch (start us, length us, event | category | flops | bytes accessed | tf_op | source)
XLA Modules:
  0.0 111.7 jit_solution(3378715373430508297)
XLA Ops:
  0.6 63.1 %scatter.1 = (bf16[96,1024]{1,0:T(8,128)(2,1)}, bf16[96,1024]{1,0:T(8,128)(2,1)}, bf16[96,512]{1,0:T(8,128)(2,1)}, bf16[96,512]{1,0:T(8,128)(2,1)}, bf16[96,16]{1,0:T(8,128)(2,1)}) custom-call(bf16[12,64,512]{2,1,0:T(8,128)(2,1)} %bitcast.19, f32[1,4096]{1,0:T(1,128)} %bitcast.27, bf16[512,1024]{1,0:T(8,128)(2,1)} %wx_ref.2, bf16[512,1024]{1,0:T(8,128)(2,1)} %wz_ref.1, ...), custom_call_target="tpu_custom_call" | custom-call | tf_op jit(solution)/shard_map/scatter/pallas_call | solution.py:421
  63.7 9.3 %mix.1 = (bf16[96,1024]{1,0:T(8,128)(2,1)}, f32[8,16,64,128]{3,2,1,0:T(8,128)}) custom-call(bf16[96,1024]{1,0:T(8,128)(2,1)} %get-tuple-element.9.x_ref, bf16[96,1024]{1,0:T(8,128)(2,1)} %get-tuple-element.10.z_ref, bf16[96,512]{1,0:T(8,128)(2,1)} %get-tuple-element.11.b_ref, bf16[96,512]{1,0:T(8,128)(2,1)} %get-tuple-element.12.c_ref, ...), custom_call_target="tpu_custom_call" | custom-call | tf_op jit(solution)/shard_map/mix/pallas_call | solution.py:653
  73.0 37.1 %project_out.1 = bf16[96,1024]{1,0:T(8,128)(2,1)} custom-call(bf16[96,1024]{1,0:T(8,128)(2,1)} %get-tuple-element.14.gated_ref, bf16[1024,512]{1,0:T(8,128)(2,1)} %w_ref.1), custom_call_target="tpu_custom_call" | custom-call | tf_op jit(solution)/shard_map/project_out/pallas_call | solution.py:976
  110.1 1.6 %copy.28 = bf16[8,12,1024]{2,0,1:T(8,128)(2,1)} copy(bf16[8,12,1024]{2,0,1:T(8,128)(2,1)} %bitcast.18) | data formatting | bytes 393216

commit v2 on v1

v2 whole, which is shorter than its diff:
```python
import functools

import jax
import jax.numpy as jnp
from jax import lax
from jax.experimental import pallas as pl
from jax.experimental.pallas import tpu as pltpu
from jax.sharding import PartitionSpec as P

HPG = 4
CORES = 2
EPS = 1e-06
HIGH = lax.Precision.HIGHEST
MESH = pl.DeviceIdType.MESH
F32 = jnp.float32
BF16 = jnp.bfloat16
LANES = 128
AHEAD = 3


def inner_size(ranks):
    return max(d for d in range(1, ranks + 1) if ranks % d == 0 and d * d <= ranks)


def dot(a, b):
    return jnp.dot(a, b, preferred_element_type=F32)


def dot_nt(a, b):
    return lax.dot_general(a, b, (((1,), (1,)), ((), ())), preferred_element_type=F32)


def dot_high(a, b):
    return jnp.dot(a, b, precision=HIGH, preferred_element_type=F32)


def silu(x):
    return x * (1.0 / (1.0 + jnp.exp(-x)))


def softplus(x):
    return jnp.maximum(x, 0.0) + jnp.log1p(jnp.exp(-jnp.abs(x)))


def iota(shape, dim):
    return lax.broadcasted_iota(jnp.int32, shape, dim)


class Stream:
    def __init__(self, index, part, near, made, pair, onward, landed):
        self.index = index
        self.part, self.near, self.made = part, near, made
        self.pair, self.onward, self.landed = pair, onward, landed


class Names:
    def __init__(self, names, refs):
        self.__dict__.update(zip(names, refs, strict=True))


def spread(values, g, lanes):
    head = lanes // HPG
    lane = iota((1, lanes), 1)
    out = values[:, HPG * g : HPG * g + 1]
    for i in range(1, HPG):
        out = jnp.where(lane >= i * head, values[:, HPG * g + i : HPG * g + i + 1], out)
    return out


def sum_of(first_term, others):
    total = first_term.astype(F32)
    for other in others:
        total = total + other.astype(F32)
    return total


def mixer_kernel(names, near, far, chunks, ratio, *refs):
    r = Names(names, refs)
    mine = lax.axis_index("kv")
    column = lax.axis_index("tp")
    blocks = lax.axis_size("tp")
    ranks = near * far
    half = far // 2
    depth = blocks // CORES
    my_far = mine // near
    my_near = lax.rem(mine, near)
    partner = my_far + 1 - 2 * lax.rem(my_far, 2)
    core = lax.rem(column, CORES)
    level = column // CORES
    owner = mine // ratio
    spot = lax.rem(mine, ratio)
    owner_level = owner // CORES
    owner_core = lax.rem(owner, CORES)
    slab = r.scaled.shape[2]
    rows = r.scaled.shape[1]
    seqs, heads, head_dim, state_dim = r.state.shape
    props = r.parents.shape[1]
    width = r.gain_in.shape[1]
    keep, path_len = r.conv_x.shape[0], r.path_x.shape[0]
    taps = keep + 1
    hrows, prows = (keep + path_len) * seqs, path_len * seqs
    xc, bc = HPG * head_dim, state_dim
    first = 2 * xc + bc
    out_slab = r.w_out.shape[1]
    low = seqs - 1
    shift = seqs.bit_length() - 1
    bc_shift = bc.bit_length() - 1

    def place(home, jump, step_near):
        return lax.rem(home + 2 * jump, far) * near + lax.rem(my_near + step_near, near)

    loads = []
    for g in range(chunks):
        at = 0
        for k, (ref, cols) in enumerate(((r.w_x, xc), (r.w_z, xc), (r.w_b, bc), (r.w_c, bc))):
            copy = pltpu.make_async_copy(
                ref.at[:, pl.ds(g * cols, cols)], r.wbuf.at[g, :, pl.ds(at, cols)], r.w_sems.at[g, k]
            )
            loads.append(copy)
            at += cols
    rate_load = pltpu.make_async_copy(
        r.w_dt.at[
            pl.ds(pl.multiple_of(column * heads, heads), heads),
            pl.ds(pl.multiple_of(mine * slab, slab), slab),
        ],
        r.wrate,
        r.w_sems.at[chunks, 0],
    )
    out_load = pltpu.make_async_copy(r.w_out, r.w_vm, r.w_sems.at[chunks, 1])
    state_loads = [
        pltpu.make_async_copy(
            r.state.at[:, pl.ds(HPG * g, HPG)], r.state_vm.at[g], r.state_sems.at[g]
        )
        for g in range(chunks)
    ]
    rate_load.start()
    for copy in loads + state_loads + [out_load]:
        copy.start()

    barrier = pltpu.get_barrier_semaphore()

    def greet(target):
        pl.semaphore_signal(barrier, inc=1, device_id=target, device_id_type=MESH)

    count = 0
    for peer in (
        [place(my_far, 0, step) for step in range(1, near)]
        + [place(partner, 0, 0)]
        + [place(my_far, jump, 0) for jump in range(1, half)]
    ):
        greet((peer, column))
        count += 1
    for other in range(1, CORES):
        greet((mine, level * CORES + lax.rem(core + other, CORES)))
        count += 1

    @pl.when(level != owner_level)
    def _():
        greet((mine, owner_level * CORES + core))

    for up in range(1, depth):

        @pl.when(level == owner_level)
        def _():
            greet((mine, lax.rem(level + up, depth) * CORES + core))

    for n in range(ratio):
        for c in range(CORES):
            source = column * ratio + n

            @pl.when(jnp.logical_or(source != mine, c != core))
            def _():
                greet((source, level * CORES + c))

    def barrier_wait():
        @pl.when(level != owner_level)
        def _():
            pl.semaphore_wait(barrier, count + 1)

        @pl.when(jnp.logical_and(level == owner_level, core != owner_core))
        def _():
            pl.semaphore_wait(barrier, count + depth - 1 + ranks)

        @pl.when(jnp.logical_and(level == owner_level, core == owner_core))
        def _():
            pl.semaphore_wait(barrier, count + depth - 1 + ranks - 1)

    copies = []
    waits = {}

    def send(key, source, landing, send_sem, recv_sem, target):
        copy = pltpu.make_async_remote_copy(
            src_ref=source,
            dst_ref=landing,
            send_sem=send_sem,
            recv_sem=recv_sem,
            device_id=(target, column),
            device_id_type=MESH,
        )
        copy.start()
        copies.append(copy)
        waits[key] = copy

    def scale_tokens():
        rate_load.wait()
        gain = r.gain_in[:, pl.ds(pl.multiple_of(mine * slab, slab), slab)]
        rate_w = r.wrate[...]

        @pl.loop(0, ranks)
        def _(d):
            tokens = r.tokens[:, pl.ds(pl.multiple_of(d * seqs, seqs), seqs), :]
            tokens = tokens.astype(F32).reshape(rows, slab)
            block = (tokens * gain).astype(BF16)
            r.scaled[d] = block
            squares = jnp.sum(tokens * tokens, axis=1, keepdims=True)
            r.side_part[d, :, 0:heads] = dot_nt(block, rate_w).astype(BF16)
            r.side_part[d, :, heads : heads + 1] = squares.astype(BF16)

    def multiply(g):
        for copy in loads[4 * g : 4 * g + 4]:
            copy.wait()

        @pl.loop(0, ranks // 2)
        def _(turn):
            block = r.scaled[pl.ds(2 * turn, 2)].reshape(2 * rows, slab)
            both = dot(block, r.wbuf[g]).astype(BF16)
            for k in range(2):
                r.part[g, 2 * turn + k] = both[k * rows : (k + 1) * rows, :first]
                r.zpart[g, 2 * turn + k] = both[k * rows : (k + 1) * rows, first:]

    order = [(jump, kind) for jump in list(range(1, half)) + [0] for kind in range(2)]
    turns = len(order)
    homes = (partner, my_far)
    side = Stream(
        chunks, r.side_part, r.side_near, r.side_made, r.side_pair, r.side_onward, r.side_far
    )
    streams = []
    for g in range(chunks):
        stream = Stream(
            g,
            r.part.at[g],
            r.near_in.at[g],
            r.made.at[g],
            r.pair_in.at[g],
            r.onward.at[g],
            r.far_in.at[g],
        )
        streams.append([side, stream] if g == 0 else [stream])

    def start_near(q):
        g, t = q // turns, q % turns
        jump, kind = order[t]
        slot = 2 * jump + kind
        for step in range(1, near):
            for s in streams[g]:
                send(
                    ("near", s.index, slot, step),
                    s.part.at[place(homes[kind], jump, step)],
                    s.near.at[slot, step - 1],
                    r.near_s.at[s.index, slot, step - 1],
                    r.near_r.at[s.index, slot, step - 1],
                    place(my_far, 0, step),
                )

    def start_zpair(g):
        for jump in list(range(1, half)) + [0]:
            for step in range(near):
                send(
                    ("zpair", g, jump, step),
                    r.zpart.at[g, place(partner, jump, step)],
                    r.zpair.at[g, jump, step],
                    r.zpair_s.at[g, jump, step],
                    r.zpair_r.at[g, jump, step],
                    place(partner, 0, 0),
                )

    def near_terms(s, slot):
        return [s.near[slot, step - 1] for step in range(1, near)]

    def reduce_step(g, t):
        jump, kind = order[t]
        slot = 2 * jump + kind
        for s in streams[g]:
            for step in range(1, near):
                waits["near", s.index, slot, step].wait_recv()
            if kind == 0:
                s.made[jump] = sum_of(
                    s.part[place(partner, jump, 0)], near_terms(s, slot)
                ).astype(BF16)
                send(
                    ("pair", s.index, jump),
                    s.made.at[jump],
                    s.pair.at[jump],
                    r.pair_s.at[s.index, jump],
                    r.pair_r.at[s.index, jump],
                    place(partner, 0, 0),
                )
            elif jump > 0:
                waits["pair", s.index, jump].wait_recv()
                s.onward[jump - 1] = sum_of(
                    s.part[place(my_far, jump, 0)], near_terms(s, slot) + [s.pair[jump]]
                ).astype(BF16)
                send(
                    ("far", s.index, jump),
                    s.onward.at[jump - 1],
                    s.landed.at[jump - 1],
                    r.far_s.at[s.index, jump - 1],
                    r.far_r.at[s.index, jump - 1],
                    place(my_far, jump, 0),
                )

    def z_onward(g):
        for jump in range(1, half):
            for step in range(near):
                waits["zpair", g, jump, step].wait_recv()
                r.zonward[g, jump - 1, step] = sum_of(
                    r.zpart[g, place(my_far, jump, step)], [r.zpair[g, jump, step]]
                ).astype(BF16)
                send(
                    ("zfar", g, jump, step),
                    r.zonward.at[g, jump - 1, step],
                    r.zfar.at[g, jump - 1, step],
                    r.zfar_s.at[g, jump - 1, step],
                    r.zfar_r.at[g, jump - 1, step],
                    place(my_far, jump, 0),
                )

    def z_terms(g, step):
        return [r.zpair[g, 0, step]] + [r.zfar[g, jump - 1, step] for jump in range(1, half)]

    def z_last(g):
        for step in range(near):
            waits["zpair", g, 0, step].wait_recv()
            for jump in range(1, half):
                waits["zfar", g, jump, step].wait_recv()
        for step in range(1, near):
            r.zfin_out[g, step - 1] = sum_of(
                r.zpart[g, place(my_far, 0, step)], z_terms(g, step)
            ).astype(BF16)
            send(
                ("zfin", g, step),
                r.zfin_out.at[g, step - 1],
                r.zfin_in.at[g, step - 1],
                r.zfin_s.at[g, step - 1],
                r.zfin_r.at[g, step - 1],
                place(my_far, 0, step),
            )

    def finish(g):
        for s in streams[g]:
            waits["pair", s.index, 0].wait_recv()
            for jump in range(1, half):
                waits["far", s.index, jump].wait_recv()
            total = sum_of(
                s.part[mine],
                near_terms(s, 1) + [s.pair[0]] + [s.landed[jump - 1] for jump in range(1, half)],
            )
            if s is side:
                scale = lax.rsqrt(total[:, heads : heads + 1] / width + EPS)
                r.scale[...] = scale
                rates(total[:, 0:heads] * scale)
            else:
                total = (total * r.scale[...]).astype(BF16)
                r.here[g, :, 0:xc] = total[:, :xc]
                r.gate[g] = total[:, xc : 2 * xc]
                r.here[g, :, xc : xc + bc] = total[:, 2 * xc :]
        for step in range(1, near):
            waits["zfin", g, step].wait_recv()
        total = sum_of(
            r.zpart[g, mine], z_terms(g, 0) + [r.zfin_in[g, step - 1] for step in range(1, near)]
        )
        r.here[g, :, xc + bc :] = (total * r.scale[...]).astype(BF16)

    bias = r.bias[...]
    a_rate = -jnp.exp(r.a_log[...])

    def tap(k, g, parts):
        held = ((r.conv_wx, xc), (r.conv_wb, bc), (r.conv_wc, bc))
        return jnp.concatenate(
            [ref[k : k + 1, g * cols : (g + 1) * cols].astype(F32) for ref, cols in held[:parts]],
            axis=1,
        )

    def accepted_column():
        eye = iota((seqs, seqs), 0) == iota((seqs, seqs), 1)
        return jnp.sum(jnp.where(eye, r.accepted[...].astype(F32), 0.0), axis=1, keepdims=True)

    def replay_weights():
        accepted = jnp.concatenate([accepted_column()] * path_len, axis=0)
        step_of = lax.shift_right_logical(iota((prows, 1), 0), shift).astype(F32)
        live = (step_of < accepted).astype(F32)
        path_step = softplus(r.path_dt[...].astype(F32).reshape(prows, heads) + bias)
        log_decay = path_step * a_rate * live
        pr, pc = iota((prows, prows), 0), iota((prows, prows), 1)
        later = jnp.where(((pr & low) == (pc & low)) & (pc > pr), 1.0, 0.0)
        every = jnp.where(iota((seqs, prows), 0) == (iota((seqs, prows), 1) & low), 1.0, 0.0)
        r.weights[...] = live * jnp.exp(dot_high(later, log_decay)) * path_step
        r.overall[...] = jnp.exp(dot_high(every, log_decay))

    def replay(g):
        at = 0
        for conv, path, cols in (
            (r.conv_x, r.path_x, xc),
            (r.conv_b, r.path_b, bc),
            (r.conv_c, r.path_c, bc),
        ):
            span = slice(g * cols, (g + 1) * cols)
            top = conv[:, :, span].astype(F32).reshape(keep * seqs, cols)
            end = path[:, :, span].astype(F32).reshape(prows, cols)
            r.hist[:, at : at + cols] = jnp.concatenate([top, end], axis=0).astype(BF16)
            at += cols
        values = r.hist[:, 0 : xc + bc].astype(F32)
        summed = tap(0, g, 2) * values[0:prows]
        for k in range(1, taps):
            summed = summed + tap(k, g, 2) * values[k * seqs : k * seqs + prows]
        post = silu(summed)
        left = (post[:, :xc] * spread(r.weights[...], g, xc)).T.astype(BF16)
        block_mask = (iota((prows, seqs * bc), 0) & low) == lax.shift_right_logical(
            iota((prows, seqs * bc), 1), bc_shift
        )
        right = jnp.where(block_mask, jnp.concatenate([post[:, xc:]] * seqs, axis=1), 0.0)
        grown = dot(left, right.astype(BF16))
        overall = r.overall[...]
        state_loads[g].wait()
        for s in range(seqs):
            for i in range(HPG):
                h = HPG * g + i
                fresh = (
                    overall[s : s + 1, h : h + 1] * r.state_vm[g, s, i]
                    + grown[i * head_dim : (i + 1) * head_dim, s * bc : (s + 1) * bc]
                )
                r.state_vm[g, s, i] = fresh
                r.new_bf[
                    g, i * head_dim : (i + 1) * head_dim, s * bc : (s + 1) * bc
                ] = fresh.astype(BF16)
        new_copy(g).start()
        reached = dot(r.all_h[...], r.hist[...])
        summed = tap(taps - 2, g, 3) * reached[0:rows]
        for k in range(2, taps):
            summed = summed + tap(taps - 1 - k, g, 3) * reached[(k - 1) * rows : k * rows]
        r.before[g] = summed

    def new_copy(g):
        return pltpu.make_async_copy(
            r.state_vm.at[g], r.new_state.at[:, pl.ds(HPG * g, HPG)], r.new_sems.at[g]
        )

    def tree():
        parents = r.parents[...].astype(F32)
        parent = jnp.concatenate([parents[:, i : i + 1] for i in range(props)], axis=0)
        accepted = jnp.concatenate([accepted_column()] * props, axis=0)
        seq_of = (iota((rows, 1), 0) & low).astype(F32)
        in_tree = parent >= 0.0
        hist_at = jnp.where(in_tree, -1.0, (accepted + (keep - 1)) * seqs + seq_of)
        prop_at = jnp.where(in_tree, parent * seqs + seq_of, -1.0)
        link_p = iota((rows, rows), 1).astype(F32) == prop_at
        link_h = iota((rows, hrows), 1).astype(F32) == hist_at
        up_p = jnp.where(link_p, 1.0, 0.0).astype(BF16)
        up_h = jnp.where(link_h, 1.0, 0.0).astype(BF16)
        back = jnp.where(
            iota((hrows, hrows), 1) == iota((hrows, hrows), 0) - seqs, 1.0, 0.0
        ).astype(BF16)
        last_p, last_h = up_p, up_h
        r.all_p[0:rows] = last_p
        r.all_h[0:rows] = last_h
        for k in range(1, taps - 1):
            last_p, last_h = (
                dot(last_p, up_p).astype(BF16),
                (dot(last_p, up_h) + dot(last_h, back)).astype(BF16),
            )
            r.all_p[k * rows : (k + 1) * rows] = last_p
            r.all_h[k * rows : (k + 1) * rows] = last_h
        self_at = iota((rows, rows), 0) == iota((rows, rows), 1)
        above = jnp.where(link_p | self_at, 1.0, 0.0)
        for _ in range((props - 1).bit_length()):
            some = above.astype(BF16)
            above = jnp.minimum(dot(some, some), 1.0)
        r.above[...] = above

    def rates(rate_rows):
        step_size = softplus(rate_rows.astype(BF16).astype(F32) + bias)
        decay = dot_high(r.above[...], step_size * a_rate)
        r.decay[...] = decay
        r.decay_t[...] = decay.T
        r.step_t[...] = step_size.T

    def mix(g):
        here = r.here[g]
        summed = r.before[g] + tap(taps - 1, g, 3) * here.astype(F32)
        reached = dot(r.all_p[...], here)
        for k in range(1, taps):
            summed = summed + tap(taps - 1 - k, g, 3) * reached[(k - 1) * rows : k * rows]
        post = silu(summed)
        post_x = post[:, :xc]
        post_b = post[:, xc : xc + bc].astype(BF16)
        post_c = post[:, xc + bc :]
        scores = dot_nt(post_c.astype(BF16), post_b)
        decay = r.decay[...]
        above = r.above[...] > 0.5
        lane = iota((1, xc), 1)
        own = (iota((rows, seqs * bc), 0) & low) == lax.shift_right_logical(
            iota((rows, seqs * bc), 1), bc_shift
        )
        wide_c = jnp.where(own, jnp.concatenate([post_c] * seqs, axis=1), 0.0).astype(BF16)
        carried = dot_nt(wide_c, r.new_bf[g])
        out = carried * spread(jnp.exp(decay), g, xc) + spread(r.skip[...], g, xc) * post_x
        for i in range(HPG):
            h = HPG * g + i
            gap = decay[:, h : h + 1] - r.decay_t[h : h + 1, :]
            mixing = jnp.where(above, jnp.exp(jnp.where(above, gap, 0.0)), 0.0)
            mixing = scores * mixing * r.step_t[h : h + 1, :]
            head = (lane >= i * head_dim) & (lane < (i + 1) * head_dim)
            out = out + dot(mixing.astype(BF16), jnp.where(head, post_x, 0.0).astype(BF16))
        out = out * silu(r.gate[g].astype(F32))
        out = out * lax.rsqrt(jnp.mean(out * out, axis=1, keepdims=True) + EPS)
        r.gathered[g, 0] = (out * r.gain_out[:, g * xc : (g + 1) * xc]).astype(BF16)

    index = {}
    for home in range(2):
        for jump in range(half):
            for step in range(near):
                index[jump, home, step] = len(index)
    sources = (my_far, partner)

    def origin(key):
        jump, home, step = key
        return lax.rem(sources[home] + far - 2 * jump, far) * near + lax.rem(
            my_near + near - step, near
        )

    def gather(g, source, key, target):
        k = index[key]
        send(
            ("gather", g, key),
            r.gathered.at[g, index[source]],
            r.gathered.at[g, k],
            r.gather_s.at[g, k],
            r.gather_r.at[g, k],
            target,
        )

    def gather_own(g):
        for jump in range(1, half):
            gather(g, (0, 0, 0), (jump, 0, 0), place(my_far, jump, 0))
        gather(g, (0, 0, 0), (0, 1, 0), place(partner, 0, 0))
        for step in range(1, near):
            gather(g, (0, 0, 0), (0, 0, step), place(my_far, 0, step))

    def gather_on(g, home, jumps):
        for jump in jumps:
            key = (jump, home, 0)
            waits["gather", g, key].wait_recv()
            if home == 0:
                gather(g, key, (jump, 1, 0), place(partner, 0, 0))
            for step in range(1, near):
                gather(g, key, (jump, home, step), place(my_far, 0, step))

    jumps = list(range(1, half))

    def gather_1(g):
        gather_on(g, 0, jumps)

    def gather_2(g):
        gather_on(g, 1, [0])

    def gather_3(g):
        gather_on(g, 1, jumps)

    def add_terms(g, keys):
        weight = r.w_vm[g * xc : (g + 1) * xc, :]
        for key in keys:
            k = index[key]
            term = dot(r.gathered[g, k], weight)
            if g > 0:
                term = r.sums[k] + term
            if g < chunks - 1:
                r.sums[k] = term
            else:
                r.terms[k] = term.astype(BF16)

    def gather_end(g):
        for home in range(2):
            for jump in range(half):
                for step in range(1, near):
                    waits["gather", g, (jump, home, step)].wait_recv()
        add_terms(g, list(index))

    arrival = [(0, 0, 0)] + [(jump, 0, 0) for jump in jumps]
    arrival += [(0, 1, 0)] + [(0, 0, step) for step in range(1, near)]
    arrival += [(jump, 1, 0) for jump in jumps]
    arrival += [(jump, 0, step) for jump in jumps for step in range(1, near)]
    arrival += [(jump, 1, step) for jump in range(half) for step in range(1, near)]
    batches = [arrival[at : at + CORES] for at in range(0, len(arrival), CORES)]

    def pick(options, which):
        out = options[0]
        for k in range(1, CORES):
            out = jnp.where(which == k, options[k], out)
        return out

    def slots(n):
        return [index[key] for key in batches[n]]

    def sibling_copy(n, other):
        target = lax.rem(core + other, CORES)
        return pltpu.make_async_remote_copy(
            src_ref=r.terms.at[pick(slots(n), target)],
            dst_ref=r.sibling_in.at[n, other - 1],
            send_sem=r.sib_s.at[n, other - 1],
            recv_sem=r.sib_r.at[n, other - 1],
            device_id=(mine, level * CORES + target),
            device_id_type=MESH,
        )

    def column_copy(n, up):
        return pltpu.make_async_remote_copy(
            src_ref=r.paired.at[n],
            dst_ref=r.column_in.at[n, up - 1],
            send_sem=r.col_s.at[n],
            recv_sem=r.col_r.at[n, up - 1],
            device_id=(mine, owner_level * CORES + core),
            device_id_type=MESH,
        )

    def done_copy(n):
        return pltpu.make_async_remote_copy(
            src_ref=r.done.at[n],
            dst_ref=r.arrived.at[spot],
            send_sem=r.done_s.at[n],
            recv_sem=r.done_r.at[spot],
            device_id=(pick([origin(key) for key in batches[n]], core), owner),
            device_id_type=MESH,
        )

    def stays(n):
        if (0, 0, 0) not in batches[n]:
            return None
        return jnp.logical_and(core == batches[n].index((0, 0, 0)), owner == column)

    def pair_up(n):
        total = r.terms[pick(slots(n), core)].astype(F32)
        for other in range(1, CORES):
            sibling_copy(n, other).wait_recv()
            total = total + r.sibling_in[n, other - 1].astype(F32)
        r.paired[n] = total.astype(BF16)
        for up in range(1, depth):

            @pl.when(lax.rem(level - owner_level + depth, depth) == up)
            def _():
                column_copy(n, up).start()

    def send_done(n):
        @pl.when(level == owner_level)
        def _():
            total = r.paired[n].astype(F32)
            for up in range(1, depth):
                column_copy(n, up).wait_recv()
                total = total + r.column_in[n, up - 1].astype(F32)
            r.done[n] = total.astype(BF16)
            here = stays(n)
            if here is None:
                done_copy(n).start()
            else:

                @pl.when(here)
                def _():
                    r.arrived[spot] = r.done[n]

                @pl.when(jnp.logical_not(here))
                def _():
                    done_copy(n).start()

    total_turns = chunks * turns
    ahead = min(AHEAD, total_turns)
    multiplied = [0]

    def near_turn(q):
        if q < total_turns:
            if q // turns > multiplied[0]:
                multiplied[0] += 1
                multiply(multiplied[0])
            start_near(q)

    scale_tokens()
    multiply(0)
    barrier_wait()
    for q in range(ahead):
        near_turn(q)
    start_zpair(0)
    tree()
    replay_weights()
    out_load.wait()
    fillers = [functools.partial(replay, g) for g in range(chunks)]
    last = chunks - 1
    for g in range(chunks):
        for t in range(turns):
            reduce_step(g, t)
            near_turn(g * turns + t + ahead)
            if t == 0:
                z_onward(g)
                if g >= 2:
                    gather_3(g - 2)
            if t == 1 and g < last:
                if g + 1 > multiplied[0]:
                    multiplied[0] += 1
                    multiply(multiplied[0])
                start_zpair(g + 1)
            if t == turns - 2:
                z_last(g)
            if g == 0 and len(fillers) > 0:
                fillers.pop(0)()
            if t == 0 and g >= 1:
                while len(fillers) > 0:
                    fillers.pop(0)()
                finish(g - 1)
                mix(g - 1)
                gather_own(g - 1)
            if t == 1 and g >= 2:
                gather_end(g - 2)
            if t == turns - 2 and g >= 1:
                gather_1(g - 1)
            if t == turns - 1 and g >= 1:
                gather_2(g - 1)
    while len(fillers) > 0:
        fillers.pop(0)()
    if last >= 1:
        gather_3(last - 1)
    finish(last)
    mix(last)
    gather_own(last)
    if last >= 1:
        gather_end(last - 1)

    for n, keys in enumerate(batches):
        for key in keys:
            if key != (0, 0, 0):
                jump, home, step = key
                if step == 0:
                    gather_on(last, home, [jump])
                else:
                    waits["gather", last, key].wait_recv()
            add_terms(last, [key])
        for other in range(1, CORES):
            sibling_copy(n, other).start()
        if n >= 1:
            pair_up(n - 1)
        if n >= 2:
            send_done(n - 2)
    final = len(batches) - 1
    pair_up(final)
    if final >= 1:
        send_done(final - 1)
    send_done(final)

    for n in range(ratio):
        source = column * ratio + n
        local = jnp.logical_and(source == mine, core == batches[0].index((0, 0, 0)))

        @pl.when(jnp.logical_not(local))
        def _():
            pltpu.make_async_remote_copy(
                src_ref=r.done.at[0],
                dst_ref=r.arrived.at[n],
                send_sem=r.done_s.at[0],
                recv_sem=r.done_r.at[n],
                device_id=(source, lax.rem(column + 1, blocks)),
                device_id_type=MESH,
            ).wait_recv()

        r.mixed[:, n * out_slab : (n + 1) * out_slab] = r.arrived[n]

    for g in range(chunks):
        new_copy(g).wait()
    for copy in copies:
        copy.wait_send()
    for n in range(len(batches)):
        for other in range(1, CORES):
            sibling_copy(n, other).wait_send()

        @pl.when(level != owner_level)
        def _():
            column_copy(n, 1).wait_send()

        @pl.when(level == owner_level)
        def _():
            here = stays(n)
            if here is None:
                done_copy(n).wait_send()
            else:

                @pl.when(jnp.logical_not(here))
                def _():
                    done_copy(n).wait_send()


def run_mixer(inputs, ranks, blocks):
    tokens, w_x, state = inputs["tokens"], inputs["w_x"], inputs["state"]
    props, all_seqs, slab = tokens.shape
    seqs, heads, head_dim, state_dim = state.shape
    rows = props * seqs
    near = inner_size(ranks)
    far = ranks // near
    half = far // 2
    chunks = heads // HPG
    ratio = ranks // blocks
    depth = blocks // CORES
    batches = ranks // CORES
    xc, bc = HPG * head_dim, state_dim
    wide = 2 * xc + bc
    out_slab = inputs["w_out"].shape[1]
    keep = inputs["conv_x"].shape[0]
    held = (keep + inputs["path_x"].shape[0]) * seqs
    prows = inputs["path_x"].shape[0] * seqs
    vmem = pl.BlockSpec(memory_space=pltpu.VMEM)
    hbm = pl.BlockSpec(memory_space=pl.ANY)
    dma = pltpu.SemaphoreType.DMA

    def buf(*shape):
        return pltpu.VMEM(shape, BF16)

    def full(*shape):
        return pltpu.VMEM(shape, F32)

    scratch = dict(
        wbuf=buf(chunks, slab, wide + bc),
        wrate=buf(heads, slab),
        w_vm=buf(w_x.shape[1], out_slab),
        scaled=buf(ranks, rows, slab),
        part=buf(chunks, ranks, rows, wide),
        near_in=buf(chunks, far, near - 1, rows, wide),
        made=buf(chunks, half, rows, wide),
        pair_in=buf(chunks, half, rows, wide),
        onward=buf(chunks, half - 1, rows, wide),
        far_in=buf(chunks, half - 1, rows, wide),
        side_part=buf(ranks, rows, LANES),
        side_near=buf(far, near - 1, rows, LANES),
        side_made=buf(half, rows, LANES),
        side_pair=buf(half, rows, LANES),
        side_onward=buf(half - 1, rows, LANES),
        side_far=buf(half - 1, rows, LANES),
        zpart=buf(chunks, ranks, rows, bc),
        zpair=buf(chunks, half, near, rows, bc),
        zonward=buf(chunks, half - 1, near, rows, bc),
        zfar=buf(chunks, half - 1, near, rows, bc),
        zfin_out=buf(chunks, near - 1, rows, bc),
        zfin_in=buf(chunks, near - 1, rows, bc),
        scale=full(rows, 1),
        here=buf(chunks, rows, xc + 2 * bc),
        gate=buf(chunks, rows, xc),
        state_vm=full(chunks, seqs, HPG, head_dim, state_dim),
        new_bf=buf(chunks, xc, seqs * bc),
        weights=full(prows, heads),
        overall=full(seqs, heads),
        hist=buf(held, xc + 2 * bc),
        before=full(chunks, rows, xc + 2 * bc),
        all_p=buf(keep * rows, rows),
        all_h=buf(keep * rows, held),
        above=full(rows, rows),
        decay=full(rows, heads),
        decay_t=full(heads, rows),
        step_t=full(heads, rows),
        gathered=buf(chunks, ranks, rows, xc),
        sums=full(ranks, rows, out_slab),
        terms=buf(ranks, rows, out_slab),
        sibling_in=buf(batches, CORES - 1, rows, out_slab),
        paired=buf(batches, rows, out_slab),
        column_in=buf(batches, depth - 1, rows, out_slab),
        done=buf(batches, rows, out_slab),
        arrived=buf(ratio, rows, out_slab),
        w_sems=dma((chunks + 1, 4)),
        state_sems=dma((chunks,)),
        new_sems=dma((chunks,)),
        near_s=dma((chunks + 1, far, near - 1)),
        near_r=dma((chunks + 1, far, near - 1)),
        pair_s=dma((chunks + 1, half)),
        pair_r=dma((chunks + 1, half)),
        far_s=dma((chunks + 1, half - 1)),
        far_r=dma((chunks + 1, half - 1)),
        zpair_s=dma((chunks, half, near)),
        zpair_r=dma((chunks, half, near)),
        zfar_s=dma((chunks, half - 1, near)),
        zfar_r=dma((chunks, half - 1, near)),
        zfin_s=dma((chunks, near - 1)),
        zfin_r=dma((chunks, near - 1)),
        gather_s=dma((chunks, ranks)),
        gather_r=dma((chunks, ranks)),
        sib_s=dma((batches, CORES - 1)),
        sib_r=dma((batches, CORES - 1)),
        col_s=dma((batches,)),
        col_r=dma((batches, depth - 1)),
        done_s=dma((batches,)),
        done_r=dma((ratio,)),
    )
    in_hbm = ("w_x", "w_z", "w_b", "w_c", "w_dt", "w_out", "state")
    names = tuple(inputs) + ("mixed", "new_state") + tuple(scratch)
    return pl.pallas_call(
        functools.partial(mixer_kernel, names, near, far, chunks, ratio),
        out_shape=(
            jax.ShapeDtypeStruct((rows, ratio * out_slab), BF16),
            jax.ShapeDtypeStruct(state.shape, F32),
        ),
        in_specs=[hbm if name in in_hbm else vmem for name in inputs],
        out_specs=(vmem, hbm),
        scratch_shapes=list(scratch.values()),
        compiler_params=pltpu.CompilerParams(collective_id=0, has_side_effects=True),
        name="mixer",
    )(*inputs.values())


def store_kernel(pieces, mixed_in, state_in, mixed_out, state_out, held, ins, outs, last):
    step = held.shape[1]
    reads, writes = [], []
    for k in range(pieces):
        reads.append(
            pltpu.make_async_copy(state_in.at[pl.ds(k * step, step)], held.at[k], ins.at[k])
        )
        writes.append(
            pltpu.make_async_copy(held.at[k], state_out.at[pl.ds(k * step, step)], outs.at[k])
        )
        reads[k].start()
    copy = pltpu.make_async_copy(mixed_in, mixed_out, last)
    copy.start()
    for k in range(pieces):
        reads[k].wait()
        writes[k].start()
    for k in range(pieces):
        writes[k].wait()
    copy.wait()


def store(mixed, state):
    pieces = state.shape[0]
    vmem = pl.BlockSpec(memory_space=pltpu.VMEM)
    hbm = pl.BlockSpec(memory_space=pl.ANY)
    dma = pltpu.SemaphoreType.DMA
    return pl.pallas_call(
        functools.partial(store_kernel, pieces),
        out_shape=(
            jax.ShapeDtypeStruct(mixed.shape, mixed.dtype),
            jax.ShapeDtypeStruct(state.shape, state.dtype),
        ),
        in_specs=[vmem, hbm],
        out_specs=(hbm, hbm),
        scratch_shapes=[
            pltpu.VMEM((pieces, state.shape[0] // pieces) + state.shape[1:], F32),
            dma((pieces,)),
            dma((pieces,)),
            dma(()),
        ],
        name="store",
    )(mixed, state)


def shards(
    tokens,
    parents,
    accepted,
    state,
    conv_x,
    conv_b,
    conv_c,
    path_x,
    path_b,
    path_c,
    path_dt,
    gain_in,
    w_x,
    w_z,
    w_b,
    w_c,
    w_dt,
    dt_bias,
    a_log,
    d_skip,
    conv_wx,
    conv_wb,
    conv_wc,
    gain_out,
    w_out,
):
    ranks = lax.axis_size("kv")
    blocks = lax.axis_size("tp")

    def front(array):
        return jnp.swapaxes(array, 0, 1)

    summed, new_state = run_mixer(
        dict(
            tokens=front(tokens),
            parents=parents,
            accepted=accepted[None, :],
            state=state,
            conv_x=front(conv_x),
            conv_b=front(conv_b),
            conv_c=front(conv_c),
            path_x=front(path_x),
            path_b=front(path_b),
            path_c=front(path_c),
            path_dt=front(path_dt),
            gain_in=gain_in[None, :],
            w_x=w_x,
            w_z=w_z,
            w_b=w_b,
            w_c=w_c,
            w_dt=w_dt.T,
            bias=dt_bias[None, :],
            a_log=a_log[None, :],
            skip=d_skip[None, :],
            conv_wx=conv_wx,
            conv_wb=conv_wb,
            conv_wc=conv_wc,
            gain_out=gain_out[None, :],
            w_out=w_out,
        ),
        ranks,
        blocks,
    )
    summed, new_state = store(summed, new_state)
    seqs, props = parents.shape
    mixed = front(summed.reshape(props, seqs, summed.shape[1]))
    return (mixed, new_state)


def solution(mesh):
    return jax.shard_map(
        shards,
        mesh=mesh,
        in_specs=(
            P(None, None, "kv"),
            P("kv", None),
            P("kv"),
            P("kv", "tp", None, None),
            P("kv", None, "tp"),
            P("kv", None, "tp"),
            P("kv", None, "tp"),
            P("kv", None, "tp"),
            P("kv", None, "tp"),
            P("kv", None, "tp"),
            P("kv", None, "tp"),
            P(),
            P("kv", "tp"),
            P("kv", "tp"),
            P("kv", "tp"),
            P("kv", "tp"),
            P(),
            P("tp"),
            P("tp"),
            P("tp"),
            P(None, "tp"),
            P(None, "tp"),
            P(None, "tp"),
            P("tp"),
            P("tp", "kv"),
        ),
        out_specs=(P("kv", None, "tp"), P("kv", "tp", None, None)),
        check_vma=False,
    )
```

time: 112 us -> 100 us (0.89)
  Pallas kernels: 109 us -> 98.2 us
  local copies, waits for them, and re-layouts: 1.62 us -> 0 us
    pallas_call x3 -> x2, Pallas kernels: 109 us -> 98.2 us  [the longest x1 93.6 us: run_mixer(): pl.pallas_call(functools.partial(mixer_kernel, names, near, far, chunks,...]
    unnamed x1 -> x0, local copies, waits for them, and re-layouts: 1.62 us -> none
where the time goes in v2:
time: 100 us; the launch traced here: 98.9 us
  Pallas kernels  98.2 us (98%)
    pallas_call x1, Pallas kernels, run_mixer(): pl.pallas_call(functools.partial(mixer_kernel, names, near, far, chunks,...  93.6 us
    pallas_call x1, Pallas kernels, store(): pl.pallas_call(functools.partial(store_kernel, pieces), out_shape=(jax.Sh...  4.58 us

profile of v2, /device:TPU:0, one launch (start us, length us, event | category | flops | bytes accessed | tf_op | source)
XLA Modules:
  0.0 98.9 jit_solution(1901935558325821870)
XLA Ops:
  0.6 93.6 %mixer.1 = (bf16[96,1024]{1,0:T(8,128)(2,1)}, f32[8,16,64,128]{3,2,1,0:T(8,128)}) custom-call(bf16[12,64,512]{2,1,0:T(8,128)(2,1)} %bitcast.18, s32[8,12]{1,0:T(8,128)} %refs_1_.1, s32[1,8]{1,0:T(1,128)} %bitcast.29, f32[8,16,64,128]{3,2,1,0:T(8,128)} %refs_3_.1, bf16[3,8,1024]{2,1,0:T(8,128)(2,1)} %bitcast.21, bf16[3,8,512]{2,1,0:T(8,128)(2,1)} %bitcast.24, ...), custom_call_target="tpu_custom_call" | custom-call | tf_op jit(solution)/shard_map/mixer/pallas_call | solution.py:896
  94.3 4.6 %store.1 = (bf16[96,1024]{1,0:T(8,128)(2,1)}, f32[8,16,64,128]{3,2,1,0:T(8,128)}) custom-call(bf16[96,1024]{1,0:T(8,128)(2,1)} %get-tuple-element.6.mixed_in, f32[8,16,64,128]{3,2,1,0:T(8,128)} %get-tuple-element.7.state_in), custom_call_target="tpu_custom_call" | custom-call | tf_op jit(solution)/shard_map/store/pallas_call | solution.py:936
